TPU v7x, 32 devices: a whole 2x2x4 slice. The times are simulated.
32 devices in a mesh: sp: 8 (over z, x), tp: 4 (over y, core).
Axes of the slice: x: 2, y: 2, z: 4, core: 2. Of those that a mesh axis runs over, the one named last changes fastest.
Arguments:
- query_logits: bfloat16 [4096, 4096], P('sp', 'tp'), may hold values from -6 to 6
- forget_logits: bfloat16 [4096, 4096], P('sp', 'tp'), may hold values from -6 to 6
- value_inputs: bfloat16 [4096, 4096], P('sp', 'tp'), may hold values from -16 to 16
- output_gate_logits: bfloat16 [4096, 4096], P('sp', 'tp'), may hold values from -6 to 6
- forget_floor_gap: float32 [4096], replicated, may hold values from 2.4414063e-05 to 0.1
- surge_log_decay: float32 [32, 4096], P('tp', 'sp'), may hold values from -0.7 to 0
- head_norm_gain: float32 [128], replicated, may hold values from 0.1 to 1.9
- output_matrix: bfloat16 [4096, 4096], P('sp', 'tp'), may hold values from -1.25 to 1.25
- branch_norm_gain: float32 [4096], replicated, may hold values from 0.1 to 1.9
- residual: bfloat16 [4096, 4096], P('sp', 'tp'), may hold values from -6 to 6
Outputs:
- output: bfloat16 [4096, 4096], P('sp', 'tp')
All inputs are finite; a program needn't handle non-finite values.
Results may differ from a plain program's by a relative error of at most 0.005.
Values may be sent and summed in bfloat16 or wider, within the bound.
No kernel may reach another device: no remote copies, remote signals or barrier semaphores. Data moves between devices by JAX's collectives and lax.ppermute only.
A program may use at most 128 MiB of HBM per device.

v0:
```python
import jax
import jax.numpy as jnp
from jax import lax
from jax.sharding import PartitionSpec as P

HEAD_DIM = 128
D = 4096
BLOCK_SPAN = 64


epsilon = 1e-06


def prefix(shard, axis, combine, identity):
    size, position = (lax.axis_size(axis), lax.axis_index(axis))
    everything = jax.tree.map(lambda part: lax.all_gather(part, axis), shard)
    start = jax.tree.map(
        lambda part, zero: jnp.broadcast_to(jnp.asarray(zero, part.dtype), part.shape),
        shard,
        identity,
    )

    def step(k, before):
        reached = k < position
        new = combine(before, jax.tree.map(lambda part: part[k], everything))
        return jax.tree.map(lambda a, b: jnp.where(reached, a, b), new, before)

    return lax.fori_loop(0, size, step, start)


def block_update(state, queries, keys_in, values_in, running):
    length = running.shape[1]
    middle = length // 2
    anchor = running[:, middle - 1 : middle, :]
    ending = running[:, -1:, :]
    causal = jnp.tril(jnp.ones((length, length), dtype=bool))
    highest = lax.Precision.HIGHEST
    inter = jnp.einsum("htd,hde->hte", queries * jnp.exp(running), state, precision=highest)
    scores = jnp.einsum(
        "htd,hsd->hts",
        queries * jnp.exp(running - anchor),
        keys_in * jnp.exp(anchor - running),
        precision=highest,
    )
    intra = jnp.einsum(
        "hts,hse->hte", jnp.where(causal[None], scores, 0.0), values_in, precision=highest
    )
    new_state = state * jnp.exp(ending[:, 0, :])[:, :, None] + jnp.einsum(
        "hsd,hse->hde", keys_in * jnp.exp(ending - running), values_in, precision=highest
    )
    return (new_state, inter + intra)


def head_gates(query_logits, forget_logits, value_inputs, gap):
    row_count = query_logits.shape[0]
    head_count = query_logits.shape[1] // HEAD_DIM

    def shaped(array):
        return array.astype(jnp.float32).reshape(row_count, head_count, HEAD_DIM)

    queries = jax.nn.silu(shaped(query_logits)) * HEAD_DIM ** (-0.5)
    keys_in = gap.reshape(head_count, HEAD_DIM) * jax.nn.sigmoid(-shaped(forget_logits))
    values_in = shaped(value_inputs)
    decay_factors = jnp.log1p(-keys_in)
    return (queries, keys_in, values_in, decay_factors)


def gated_norm(heads_out, output_gate_logits, head_norm_gain):
    mean_sq = jnp.mean(heads_out * heads_out, axis=-1, keepdims=True)
    gates = jax.nn.silu(output_gate_logits.astype(jnp.float32).reshape(heads_out.shape))
    normed = heads_out * lax.rsqrt(mean_sq + epsilon) * head_norm_gain * gates
    return normed.reshape(heads_out.shape[0], -1).astype(jnp.bfloat16)


def combine(earlier, later):
    return (earlier[0] * later[0], later[0][:, :, None] * earlier[1] + later[1])


def per_device(
    query_logits,
    forget_logits,
    value_inputs,
    output_gate_logits,
    forget_floor_gap,
    surge_log_decay,
    head_norm_gain,
    output_matrix,
    branch_norm_gain,
    residual,
):
    row_count = query_logits.shape[0]
    head_cols = query_logits.shape[1]
    head_count = head_cols // HEAD_DIM
    number_of_blocks = row_count // BLOCK_SPAN
    column = lax.axis_index("tp")
    whole_weight = lax.all_gather(output_matrix, "sp", axis=0, tiled=True)
    gap = lax.dynamic_slice_in_dim(forget_floor_gap, column * head_cols, head_cols)
    queries, keys_in, values_in, decay_factors = head_gates(
        query_logits, forget_logits, value_inputs, gap
    )
    decay_factors = decay_factors + jnp.transpose(surge_log_decay)[:, :, None]

    def to_blocks(array):
        return array.reshape(number_of_blocks, BLOCK_SPAN, head_count, HEAD_DIM).transpose(
            0, 2, 1, 3
        )

    queries = to_blocks(queries)
    running = jnp.cumsum(to_blocks(decay_factors), axis=2)

    def step_forward(state, input_tuple):
        return block_update(state, input_tuple[0], input_tuple[1], input_tuple[2], input_tuple[3])

    starting_state = jnp.zeros((head_count, HEAD_DIM, HEAD_DIM), jnp.float32)
    end_state, local_out = lax.scan(
        step_forward, starting_state, (queries, to_blocks(keys_in), to_blocks(values_in), running)
    )
    totals = running[:, :, -1, :]
    before = jnp.cumsum(totals, axis=0) - totals
    whole_decay = jnp.exp(jnp.sum(totals, axis=0))
    identity = (jnp.ones_like(whole_decay), jnp.zeros_like(end_state))
    unused_slot, carried = prefix((whole_decay, end_state), "sp", combine, identity)
    reach = queries * jnp.exp(running + before[:, :, None, :])
    heads_out = local_out + jnp.einsum(
        "nhtd,hde->nhte", reach, carried, precision=lax.Precision.HIGHEST
    )
    heads_out = heads_out.transpose(0, 2, 1, 3).reshape(row_count, head_count, HEAD_DIM)
    mixed_rows = gated_norm(heads_out, output_gate_logits, head_norm_gain)
    all_heads = lax.all_gather(mixed_rows, "tp", axis=1, tiled=True)
    projected = jnp.dot(all_heads, whole_weight, preferred_element_type=jnp.float32)
    branch = lax.optimization_barrier(projected.astype(jnp.bfloat16)).astype(jnp.float32)
    squares = lax.psum(jnp.sum(branch * branch, axis=1), "tp")
    scale = lax.rsqrt(squares / D + epsilon)
    out_cols = branch.shape[1]
    gain_part = lax.dynamic_slice_in_dim(branch_norm_gain, column * out_cols, out_cols)
    return (residual.astype(jnp.float32) + branch * scale[:, None] * gain_part).astype(jnp.bfloat16)


def solution(mesh):
    placed = (
        P("sp", "tp"),
        P("sp", "tp"),
        P("sp", "tp"),
        P("sp", "tp"),
        P(),
        P("tp", "sp"),
        P(),
        P("sp", "tp"),
        P(),
        P("sp", "tp"),
    )
    return jax.shard_map(
        per_device, mesh=mesh, in_specs=placed, out_specs=P("sp", "tp"), check_vma=False
    )
```

profile of v0, /device:TPU:0, one launch (start us, length us, event | category | flops | bytes accessed | tf_op | source)
XLA Modules:
  0.0 348.8 jit_solution(4762647425927424889)
XLA Ops:
  7.4 1.8 divide_bitcast_fusion
  9.2 1.8 copy.48
  13.2 1.5 bitcast_bitcast_fusion
  14.6 4.0 %fusion.36 = f32[8,8,64,128]{3,1,2,0:T(8,128)} fusion(f32[8,64,8]{2,1,0:T(8,128)S(1)} %bitcast.184, f32[8,128]{1,0:T(8,128)S(1)} %dynamic-slice_bitcast_fusion.1, f32[8,64,8,128]{3,2,1,0:T(8,128)} %bitcast.177), kind=kOutput, calls=%fused_computation.60 | output fusion | flops 34603008 | bytes 4214784 | tf_op jit(solution)/shard_map/jit(cumsum)/reduce_window_sum | solution.py:109
  18.6 2.5 fusion.34
  21.1 47.1 %while.27 = (s32[]{:T(128)}, f32[8,128,128]{2,1,0:T(8,128)S(1)}, f32[8,8,64,128]{3,2,0,1:T(8,128)}, f32[8,8,64,128]{3,1,2,0:T(8,128)}, f32[8,8,64,128]{3,1,2,0:T...) while((s32[]{:T(128)}, f32[8,128,128]{2,1,0:T(8,128)S(1)}, ...), condition=%wide.region_2.3_spmd.clone, body=%wide.region_1.2_spmd.clone.sunk | while | flops 303075328 | bytes 7647356 | solution.py:115
  24.1 1.2 convolution_add_fusion.3
  35.8 1.2 convolution_add_fusion.3
  41.7 1.2 convolution_add_fusion.3
  43.5 1.2 fusion.74
  47.6 1.2 convolution_add_fusion.3
  53.5 1.2 convolution_add_fusion.3
  69.9 33.1 %all-gather = f32[64,128]{1,0:T(8,128)S(1)} all-gather(f32[8,128]{1,0:T(8,128)S(1)} %exp.52), channel_id=2, replica_groups=mesh['sp'=8,'tp'=4] {'sp'}, dimensions={0}, use_global_device_ids=true | all-gather | bytes 36864 | tf_op jit(solution)/shard_map/all_gather | solution.py:16
  103.9 3.8 %exponential_multiply_fusion = f32[8,8,64,128]{3,1,2,0:T(8,128)} fusion(f32[8,8,64,128]{3,1,2,0:T(8,128)} %get-tuple-element.376, f32[8,8,128]{2,1,0:T(8,128)S(1)} %fusion.47, f32[8,64,8,128]{3,2,1,0:T(8,128)S(1)} %bitcast.176), kind=kLoop, calls=%fused_computation.67 | loop fusion | flops 3670016 | bytes 6324224 | tf_op jit(solution)/shard_map/mul | solution.py:123
  107.7 37.2 %all-gather.10.cloned.1.call-done = f32[64,128,128]{2,1,0:T(8,128)} async-done(((f32[8,128,128]{2,1,0:T(8,128)}), f32[64,128,128]{2,1,0:T(8,128)}) %all-gather.10.cloned.1.call-update) | async-done | bytes 4194320 | tf_op jit(solution)/shard_map/all_gather | solution.py:16
  144.9 11.4 %while.28 = (s32[]{:T(128)}, f32[8,128,128]{2,1,0:T(8,128)S(1)}, s32[]{:T(128)}, f32[8,8,128]{2,1,0:T(8,128)S(1)}, f32[8,8,128,128]{3,2,1,0:T(8,128)}, /*index=5*/s32[]{:T(128)}, s32[]{:T(128)}) while((s32[]{:T(128)}, f32[8,128,128]{2,1,0:T(8,128)S(1)}, s32[]{:T(128)}, f32[8,8,128]{2,1,0:T(8,128)S(1)}, ...), condition=%wide.region_5.6_spmd.clone, body=%wide.region_4.5_spmd.clone.sunk | while | flops 524292 | bytes 1585265 | solution.py:28
  144.9 1.4 fusion.75
  146.3 1.4 fusion.75
  147.8 1.4 fusion.75
  149.2 1.4 fusion.75
  150.6 1.4 fusion.75
  152.0 1.4 fusion.75
  153.5 1.4 fusion.75
  154.9 1.4 fusion.75
  156.3 4.7 %multiply_reduce_fusion = (f32[8,64,8]{1,0,2:T(8,128)S(1)}, f32[8,64,8,128]{3,1,0,2:T(8,128)S(1)}) fusion(f32[8,8,64,128]{3,2,0,1:T(8,128)} %get-tuple-element.137, f32[8,8,64,128]{3,1,2,0:T(8,128)} %exponential_multiply_fusion, f32[8,128,128]{2,1,0:T(8,128)S(1)} %get-tuple-element.139), kind=kOutput, calls=%fused_computation.66 | convolution fusion | flops 806875136 | bytes 6832128 | tf_op jit(solution)/shard_map/nhtd,hde->nhte/dot_general | solution.py:124
  161.1 1.2 copy.32
  163.5 2.2 fusion.43
  166.6 32.4 %all-gather.6.cloned.1.call-done = bf16[512,4096]{1,0:T(8,128)(2,1)} async-done(((bf16[512,1024]{1,0:T(8,128)(2,1)}), bf16[512,4096]{1,0:T(8,128)(2,1)}) %all-gather.6.cloned.1.call-update) | async-done | bytes 4194320 | tf_op jit(solution)/shard_map/all_gather | solution.py:129
  199.0 126.6 %all-gather.8.cloned.1.call-done = bf16[4096,1024]{1,0:T(8,128)(2,1)} async-done(((bf16[512,1024]{1,0:T(8,128)(2,1)}), bf16[4096,1024]{1,0:T(8,128)(2,1)}) %all-gather.8.cloned.1.call-update) | async-done | bytes 8388624 | tf_op jit(solution)/shard_map/all_gather | solution.py:96
  325.6 9.1 %convolution_convert_fusion = bf16[512,1024]{1,0:T(8,128)(2,1)S(1)} fusion(bf16[512,4096]{1,0:T(8,128)(2,1)} %all-gather.6.cloned.1.call-done, bf16[4096,1024]{1,0:T(8,128)(2,1)} %all-gather.8.cloned.1.call-done), kind=kOutput, calls=%fused_computation.74 | convolution fusion | flops 4295491584 | bytes 13631488 | tf_op jit(solution)/shard_map/dot_general | solution.py:130
  335.0 5.9 %psum.7 = f32[512]{0:T(512)S(1)} all-reduce(f32[512]{0:T(512)S(1)} %fusion.25), channel_id=1, replica_groups=mesh['sp'=8,'tp'=4] {'tp'}, use_global_device_ids=true, to_apply=%region_9.10 | all-reduce | flops 512 | bytes 4096 | tf_op jit(solution)/shard_map/psum | solution.py:132
  340.9 1.4 fusion.28
  (124 shorter events, 47.6 us)
Async XLA Ops:
  6.5 8.1 %copy-start = (f32[4096]{0:T(1024)S(1)}, f32[4096]{0:T(1024)}, u32[]{:S(2)}) copy-start(f32[4096]{0:T(1024)} %param.18) | copy-start | bytes 49156
  6.5 138.4 %all-gather.10.cloned.1.call-start = ((), (), s32[]{:S(2)}) async-start(), calls=%async_computation.2 | async-start | bytes 4718592 | tf_op jit(solution)/shard_map/all_gather | solution.py:16
  9.2 1.8 copy-start.3
  11.2 1.2 copy-start.4
  14.6 4.0 %copy-start.2 = (f32[64,8,8,128]{3,2,1,0:T(8,128)S(1)}, f32[64,8,8,128]{3,2,1,0:T(8,128)}, u32[]{:S(2)}) copy-start(f32[64,8,8,128]{3,2,1,0:T(8,128)} %copy.48) | copy-start | bytes 6291460
  21.1 81.9 %copy-start.7 = (f32[128]{0:T(128)S(1)}, f32[128]{0:T(128)}, u32[]{:S(2)}) copy-start(f32[128]{0:T(128)} %param.20) | copy-start | bytes 1540
  68.2 0.8 copy-start.1
  69.0 129.9 %all-gather.6.cloned.1.call-start = ((), (), s32[]{:S(2)}) async-start(), calls=%async_computation | async-start | bytes 5242880 | tf_op jit(solution)/shard_map/all_gather | solution.py:129
  162.3 1.2 copy-start.6
  165.8 159.8 %all-gather.8.cloned.1.call-start = ((), (), s32[]{:S(2)}) async-start(), calls=%async_computation.1 | async-start | bytes 9437184 | tf_op jit(solution)/shard_map/all_gather | solution.py:96
  166.5 174.3 %copy-start.5 = (bf16[512,1024]{1,0:T(8,128)(2,1)S(1)}, bf16[512,1024]{1,0:T(8,128)(2,1)}, u32[]{:S(2)}) copy-start(bf16[512,1024]{1,0:T(8,128)(2,1)} %param.23) | copy-start | bytes 3145732
  166.6 174.3 %dynamic-slice-start = ((f32[4096]{0:T(1024)}, s32[]{:T(128)}), f32[1024]{0:T(1024)S(1)}, s32[]{:S(2)}) async-start(f32[4096]{0:T(1024)} %param.22, s32[]{:T(128)} %select_n.32), calls=%async_computation.3 | async-start | bytes 8704 | tf_op jit(solution)/shard_map/dynamic_slice | solution.py:135
Sparse Core Ops, SparseCore 0:
  69.2 75.6 all-gather.9
  165.9 32.9 all-gather.5
  201.1 124.4 all-gather.7
where the time goes:
time: 350 us; the launch traced here: 349 us
  waiting for transfers between devices  197 us (56%)
  matrix products  42.7 us (12%)
  blocking collectives  39 us (11%)
  other arithmetic  29.2 us (8%)
  local copies, waits for them, and re-layouts  26.9 us (8%)
  between operations  13.3 us (4%)
    all_gather x1, waiting for transfers between devices, per_device(): whole_weight = lax.all_gather(output_matrix, 'sp', axis=0, tiled=True)  127 us
    all_gather x1, waiting for transfers between devices, prefix(): everything = jax.tree.map(lambda part: lax.all_gather(part, axis), shard)  37.2 us
    all_gather x1, blocking collectives, prefix(): everything = jax.tree.map(lambda part: lax.all_gather(part, axis), shard)  33.1 us
    all_gather x1, waiting for transfers between devices, per_device(): all_heads = lax.all_gather(mixed_rows, 'tp', axis=1, tiled=True)  32.4 us
    dynamic_slice x24, local copies, waits for them, and re-layouts, per_device(): lax.scan(step_forward, starting_state, (queries, to_blocks(keys_in), to_b...  17.5 us
    select_n x8, other arithmetic, step(): return jax.tree.map(lambda a, b: jnp.where(reached, a, b), new, before)  11 us
    dot_general x8, matrix products, block_update(): jnp.einsum('hsd,hse->hde', keys_in * jnp.exp(ending - running), values_in...  9.24 us
    dot_general x1, matrix products, per_device(): jnp.dot(all_heads, whole_weight, preferred_element_type=jnp.float32)  9.14 us
  transfers between devices with their start and end apart: 3, of which 3 were waited for; matrix products, arithmetic and copies ran while one was open for 2% of the time, Pallas kernels for 0%

commit v1 on v0

v1 whole, which is shorter than its diff:
```python
import functools

import jax
import jax.numpy as jnp
from jax import lax
from jax.experimental import pallas as pl
from jax.experimental.pallas import tpu as pltpu
from jax.sharding import PartitionSpec as P


HEAD_DIM = 128
SPAN = 128
EXTRA = 8
TILE = 256
epsilon = 1e-06


f32 = jnp.float32
bf16 = jnp.bfloat16
NN = (((1,), (0,)), ((), ()))
TN = (((0,), (0,)), ((), ()))
NT = (((1,), (1,)), ((), ()))


def dot(a, b, dims=NN):
    return lax.dot_general(a, b, dims, preferred_element_type=f32)


def split2(value):
    high = value.astype(bf16)
    return high, (value - high.astype(f32)).astype(bf16)


def input_gate(forget_logits, gap):
    return gap / (1.0 + jnp.exp(forget_logits.astype(f32)))


def pack_decay(decay):
    first, _ = split2(decay)
    second, third = split2(decay - first.astype(f32))
    rows = [t.astype(f32) for t in (first, second, third)]
    row = lax.broadcasted_iota(jnp.int32, (EXTRA, decay.shape[-1]), 0)
    out = jnp.where(row == 2, rows[2], 0.0)
    return jnp.where(row == 0, rows[0], jnp.where(row == 1, rows[1], out)).astype(bf16)


def unpack(ref, head):
    state = ref[head, :HEAD_DIM, :].astype(f32)
    decay = jnp.sum(ref[head, HEAD_DIM:, :].astype(f32), axis=0, keepdims=True)
    return state, decay


def states_kernel(first_ref, tp_ref, forget_ref, value_ref, surge_ref, gap_ref, running_ref, packed_ref, column_ref):
    step = pl.program_id(0)
    per = packed_ref.shape[0]
    rows = forget_ref.shape[0]

    @pl.when(step == 0)
    def _():
        column_ref[...] = jnp.transpose(surge_ref[...])

    column = lax.broadcasted_iota(jnp.int32, (SPAN, 2 * SPAN), 1) % SPAN
    lower = (column <= lax.broadcasted_iota(jnp.int32, (SPAN, 2 * SPAN), 0)).astype(bf16)
    surges = column_ref[...]
    lane = lax.broadcasted_iota(jnp.int32, surges.shape, 1)
    for i in range(per):
        cols = slice(i * HEAD_DIM, (i + 1) * HEAD_DIM)
        head = (first_ref[0] + step) * per + i
        gates = input_gate(forget_ref[:, cols], gap_ref[i])
        surge = jnp.sum(jnp.where(lane == head, surges, 0.0), axis=1, keepdims=True)
        high, low = split2(jnp.log1p(-gates) + surge)
        after = jnp.zeros((1, HEAD_DIM), f32)
        keys = []
        for start in reversed(range(0, rows, SPAN)):
            part = slice(start, start + SPAN)
            running = dot(lower, jnp.concatenate([high[part], low[part]], axis=0))
            running_ref[part, cols] = running
            after = after + running[SPAN - 1 :, :]
            keys.append((gates[part] * jnp.exp(after - running)).astype(bf16))
        keys = jnp.concatenate(keys[::-1], axis=0)
        packed_ref[i, :HEAD_DIM, :] = dot(value_ref[:, cols], keys, TN).astype(bf16)
        packed_ref[i, HEAD_DIM:, :] = pack_decay(jnp.exp(after))


def local_kernel(first_ref, tp_ref, query_ref, forget_ref, value_ref, running_ref, gap_ref, local_ref, reach_ref):
    rows = query_ref.shape[0]
    row = lax.broadcasted_iota(jnp.int32, (SPAN, SPAN), 0)
    causal = lax.broadcasted_iota(jnp.int32, (SPAN, SPAN), 1) <= row
    for i in range(query_ref.shape[1] // HEAD_DIM):
        cols = slice(i * HEAD_DIM, (i + 1) * HEAD_DIM)
        before = jnp.zeros((1, HEAD_DIM), f32)
        state = None
        for start in range(0, rows, SPAN):
            part = slice(start, start + SPAN)
            logits = query_ref[part, cols].astype(f32)
            queries = logits / (1.0 + jnp.exp(-logits)) * HEAD_DIM**-0.5
            gates = input_gate(forget_ref[part, cols], gap_ref[i])
            values = value_ref[part, cols]
            running = running_ref[part, cols]
            anchor = running[SPAN // 2 - 1 : SPAN // 2, :]
            total = running[SPAN - 1 :, :]
            late = (queries * jnp.exp(running - anchor)).astype(bf16)
            early = (gates * jnp.exp(anchor - running)).astype(bf16)
            scores = jnp.where(causal, dot(late, early, NT), 0.0).astype(bf16)
            out = dot(scores, values)
            faded = queries * jnp.exp(running)
            if state is not None:
                out = out + dot(faded.astype(bf16), state.astype(bf16), NT)
            local_ref[part, cols] = out
            reach_ref[part, cols] = (faded * jnp.exp(before)).astype(bf16)
            if start + SPAN < rows:
                keys = (gates * jnp.exp(total - running)).astype(bf16)
                fresh = dot(values, keys, TN)
                state = fresh if state is None else state * jnp.exp(total) + fresh
                before = before + total


def pair_kernel(odd_ref, own_ref, other_ref, out_ref):
    even = odd_ref[0] == 0
    for head in range(own_ref.shape[0]):
        own, own_decay = unpack(own_ref, head)
        other, other_decay = unpack(other_ref, head)
        mine = jnp.where(even, other_decay, 1.0)
        theirs = jnp.where(even, 1.0, own_decay)
        out_ref[head, :HEAD_DIM, :] = (own * mine + other * theirs).astype(bf16)
        out_ref[head, HEAD_DIM:, :] = pack_decay(own_decay * other_decay)


def combine_kernel(earlier_ref, later_ref, out_ref):
    for head in range(later_ref.shape[0]):
        early, early_decay = unpack(earlier_ref, head)
        late, late_decay = unpack(later_ref, head)
        out_ref[head, :HEAD_DIM, :] = (early * late_decay + late).astype(bf16)
        out_ref[head, HEAD_DIM:, :] = pack_decay(early_decay * late_decay)


def carry_kernel(odd_ref, earlier_ref, later_ref, own_ref, other_ref, mine_ref, theirs_ref):
    odd = odd_ref[0] == 1
    for head in range(own_ref.shape[0]):
        early, _ = unpack(earlier_ref, head)
        late, late_decay = unpack(later_ref, head)
        before = early * late_decay + late
        own, own_decay = unpack(own_ref, head)
        other, other_decay = unpack(other_ref, head)
        first = jnp.where(odd, other, own)
        decay = jnp.where(odd, other_decay, own_decay)
        after = before * decay + first
        mine_ref[head] = jnp.where(odd, after, before).astype(bf16)
        theirs_ref[head] = jnp.where(odd, before, after).astype(bf16)


def mix_kernel(first_ref, local_ref, reach_ref, carried_ref, gate_ref, gain_ref, out_ref):
    for i in range(carried_ref.shape[0]):
        cols = slice(i * HEAD_DIM, (i + 1) * HEAD_DIM)
        heads_out = local_ref[:, cols] + dot(reach_ref[:, cols], carried_ref[i], NT)
        mean_sq = jnp.mean(heads_out * heads_out, axis=1, keepdims=True)
        logits = gate_ref[:, cols].astype(f32)
        gates = logits / (1.0 + jnp.exp(-logits))
        mixed = heads_out * lax.rsqrt(mean_sq + epsilon) * gain_ref[...] * gates
        out_ref[:, cols] = mixed.astype(bf16)


def ring_at(place, size):
    return jnp.where(place < size // 2, 2 * place, 2 * (size - 1 - place) + 1)


def place_of(member, size):
    return jnp.where(member % 2 == 0, member // 2, size - 1 - member // 2)


def near_kernel(sp_ref, tp_ref, *refs, offsets, size, n_mixed):
    mixed = refs[:n_mixed]
    chunks = refs[n_mixed:-2]
    out_ref, table = refs[-2:]
    at = place_of(sp_ref[0], size)
    per = 2

    @pl.when(pl.program_id(0) == 0)
    def _():
        for i, piece in enumerate(mixed):
            group = (i + sp_ref[0]) % 2
            table[(tp_ref[0] ^ (i // per)) * per + group] = piece[...]

    total = None
    half = chunks[0].shape[0]
    for i, offset in enumerate(offsets):
        block = ring_at((at + (offset + size)) % size, size)
        for j in range(2):
            part = dot(table[block, :, j * half : (j + 1) * half], chunks[2 * i + j][...])
            total = part if total is None else total + part
    out_ref[...] = total


def far_kernel(sp_ref, *refs, offsets, size):
    table, partial_ref = refs[:2]
    chunks = refs[2:-1]
    out_ref = refs[-1]
    at = place_of(sp_ref[0], size)
    total = partial_ref[...]
    half = chunks[0].shape[0]
    for i, offset in enumerate(offsets):
        block = ring_at((at + (offset + size)) % size, size)
        for j in range(2):
            total = total + dot(table[block, :, j * half : (j + 1) * half], chunks[2 * i + j][...])
    out_ref[...] = total


def last_kernel(sp_ref, table, partial_ref, first_ref, second_ref, out_ref, square_ref, lanes_ref, *, size):
    del sp_ref
    half = first_ref.shape[0]
    total = partial_ref[...] + dot(table[0, :, :half], first_ref[...])
    total = total + dot(table[0, :, half:], second_ref[...])
    rounded = total.astype(bf16)
    out_ref[...] = rounded
    wide = rounded.astype(f32)
    squares = wide * wide
    lanes = squares[:, :128]
    for start in range(128, squares.shape[1], 128):
        lanes = lanes + squares[:, start : start + 128]

    @pl.when(pl.program_id(0) == 0)
    def _():
        lanes_ref[...] = lanes

    @pl.when(pl.program_id(0) > 0)
    def _():
        lanes_ref[...] += lanes

    @pl.when(pl.program_id(0) == pl.num_programs(0) - 1)
    def _():
        high, low = split2(lanes_ref[...])
        ones = jnp.ones((8, 128), bf16)
        square_ref[...] = (dot(ones, high, NT) + dot(ones, low, NT))[:1]


def norm_kernel(tp_ref, square_ref, projected_ref, residual_ref, gain_ref, out_ref, *, width):
    squares = jnp.broadcast_to(square_ref[...], (8, square_ref.shape[1]))
    scale = lax.rsqrt(jnp.transpose(squares)[:, :1] / width + epsilon)
    branch = projected_ref[...].astype(f32) * scale * gain_ref[...]
    out_ref[...] = (residual_ref[...].astype(f32) + branch).astype(bf16)


def vmem():
    return pl.BlockSpec(memory_space=pltpu.VMEM)


def smem():
    return pl.BlockSpec(memory_space=pltpu.SMEM)


def call(kernel, scalars, operands, out_shape, grid, in_specs, out_specs, scratch=()):
    spec = pltpu.PrefetchScalarGridSpec(
        num_scalar_prefetch=len(scalars),
        grid=grid,
        in_specs=in_specs,
        out_specs=out_specs,
        scratch_shapes=list(scratch),
    )
    return pl.pallas_call(kernel, grid_spec=spec, out_shape=out_shape)(*scalars, *operands)


def permute(array, axis, pairs):
    return lax.ppermute(array, axis, pairs)


def is_ringed(sp, tp):
    return sp == 2 * tp and sp <= 8


def ring_gather(own, axis):
    size = lax.axis_size(axis)
    ring = list(range(0, size, 2)) + list(range(1, size, 2))[::-1]
    forward = [(ring[i], ring[(i + 1) % size]) for i in range(size)]
    backward = [(b, a) for a, b in forward]
    half = own.shape[0] // 2
    chunks = {0: (own[:half], own[half:])}
    for step in range(1, size // 2):
        chunks[-step], chunks[step] = [None, None], [None, None]
        for part in range(2):
            for sign, pairs in ((-1, forward), (1, backward)):
                chunks[sign * step][part] = permute(chunks[sign * (step - 1)][part], axis, pairs)
    last = size // 2
    chunks[last] = (permute(chunks[1 - last][0], axis, forward), permute(chunks[last - 1][1], axis, backward))
    return chunks


def swap(array, axis, bit):
    size = lax.axis_size(axis)
    return permute(array, axis, [(i, i ^ bit) for i in range(size)])


def shift(array, axis, by):
    size = lax.axis_size(axis)
    return permute(array, axis, [(i, i + by) for i in range(size - by)])


def carried_states(given, kept, axis, odd):
    size = lax.axis_size(axis)
    like = jax.ShapeDtypeStruct(kept.shape, kept.dtype)
    other = swap(given, axis, 1)
    pair = pl.pallas_call(pair_kernel, out_shape=like, in_specs=[smem(), vmem(), vmem()], out_specs=vmem(), name="pair")(odd, kept, other)

    def combine(earlier, later):
        return pl.pallas_call(combine_kernel, out_shape=like, in_specs=[vmem(), vmem()], out_specs=vmem(), name="combine")(earlier, later)

    earlier, later = shift(pair, axis, 2), None
    reach = 2
    while reach < size // 2:
        before = earlier if later is None else combine(earlier, later)
        earlier, later = shift(combine(before, pair), axis, 2 * reach), before
        reach *= 2
    state = jax.ShapeDtypeStruct((kept.shape[0], HEAD_DIM, HEAD_DIM), bf16)
    mine, theirs = pl.pallas_call(
        carry_kernel,
        out_shape=(state, state),
        in_specs=[smem()] + [vmem()] * 4,
        out_specs=(vmem(), vmem()),
        name="carry",
    )(odd, earlier, later, kept, other)
    return mine, swap(theirs, axis, 1)


def layer(
    query_logits,
    forget_logits,
    value_inputs,
    output_gate_logits,
    forget_floor_gap,
    surge_log_decay,
    head_norm_gain,
    output_matrix,
    branch_norm_gain,
    residual,
):
    rows, head_cols = query_logits.shape
    heads = head_cols // HEAD_DIM
    sp, tp = lax.axis_size("sp"), lax.axis_size("tp")
    sp_at = lax.axis_index("sp").astype(jnp.int32).reshape(1)
    tp_at = lax.axis_index("tp").astype(jnp.int32).reshape(1)
    odd = sp_at % 2
    width = output_matrix.shape[0] * sp
    out_cols = output_matrix.shape[1]
    ringed = is_ringed(sp, tp)

    if ringed:
        chunks = ring_gather(output_matrix, "sp")
    else:
        whole_weight = lax.all_gather(output_matrix, "sp", axis=0, tiled=True)

    group = heads // 2
    per = 2
    steps = group // per
    gap = forget_floor_gap.reshape(-1, 1, HEAD_DIM)
    block = pl.BlockSpec((rows, per * HEAD_DIM), lambda s, first, at: (0, first[0] + s))
    own_block = pl.BlockSpec((rows, per * HEAD_DIM), lambda s, first, at: (0, s))
    gap_block = pl.BlockSpec((per, 1, HEAD_DIM), lambda s, first, at: (at[0] * (heads // per) + first[0] + s, 0, 0))
    wide = jax.ShapeDtypeStruct((rows, group * HEAD_DIM), f32)
    narrow = jax.ShapeDtypeStruct((rows, group * HEAD_DIM), bf16)

    def group_states(first):
        return call(
            states_kernel,
            (first, tp_at),
            (forget_logits, value_inputs, surge_log_decay, gap),
            (wide, jax.ShapeDtypeStruct((group, HEAD_DIM + EXTRA, HEAD_DIM), bf16)),
            (steps,),
            [block, block, pl.BlockSpec((heads, rows), lambda s, first, at: (0, 0)), gap_block],
            (own_block, pl.BlockSpec((per, HEAD_DIM + EXTRA, HEAD_DIM), lambda s, first, at: (s, 0, 0))),
            [pltpu.VMEM((rows, heads), f32)],
        )

    def group_local(first, running):
        return call(
            local_kernel,
            (first, tp_at),
            (query_logits, forget_logits, value_inputs, running, gap),
            (wide, narrow),
            (steps,),
            [block, block, block, own_block, gap_block],
            (own_block, own_block),
        )

    def group_mix(first, local, reach, carried):
        shared = pl.BlockSpec((rows, per * HEAD_DIM), lambda s, first: (0, s))
        return call(
            mix_kernel,
            (first,),
            (local, reach, carried, output_gate_logits, head_norm_gain.reshape(1, HEAD_DIM)),
            narrow,
            (steps,),
            [
                shared,
                shared,
                pl.BlockSpec((per, HEAD_DIM, HEAD_DIM), lambda s, first: (s, 0, 0)),
                pl.BlockSpec((rows, per * HEAD_DIM), lambda s, first: (0, first[0] + s)),
                pl.BlockSpec((1, HEAD_DIM), lambda s, first: (0, 0)),
            ],
            shared,
        )

    given_first, kept_first = (1 - odd) * steps, odd * steps
    given_running, given = group_states(given_first)
    kept_running, kept = group_states(kept_first)
    mine, others = carried_states(given, kept, "sp", odd)
    kept_local = group_local(kept_first, kept_running)
    given_local = group_local(given_first, given_running)
    pieces = {0: [group_mix(kept_first, *kept_local, mine), group_mix(given_first, *given_local, others)]}
    bit = tp // 2
    while bit:
        for rel in sorted(pieces):
            pieces[rel ^ bit] = [swap(piece, "tp", bit) for piece in pieces[rel]]
        bit //= 2
    mixed = [piece for rel in range(tp) for piece in pieces[rel]]

    tile = min(TILE, out_cols)
    grid = (out_cols // tile,)
    if ringed:
        last = sp // 2
        cols = group * HEAD_DIM
        chunk = cols // 2
        partial_sum = jax.ShapeDtypeStruct((rows, out_cols), f32)
        piece_spec = lambda: pl.BlockSpec((rows, cols), lambda n, *_: (0, 0))
        slab = pl.BlockSpec((chunk, tile), lambda n, *_: (0, n))
        sheet = pl.BlockSpec((rows, tile), lambda n, *_: (0, n))
        whole_table = pl.BlockSpec((sp, rows, cols), lambda n, *_: (0, 0, 0))
        near = [0] + [s * k for k in range(1, last - 1) for s in (-1, 1)]
        far = [s * (last - 1) for s in (-1, 1)]
        partial, table = call(
            functools.partial(near_kernel, offsets=near, size=sp, n_mixed=len(mixed)),
            (sp_at, tp_at),
            (*mixed, *[half for off in near for half in chunks[off]]),
            (partial_sum, jax.ShapeDtypeStruct((sp, rows, cols), bf16)),
            grid,
            [piece_spec()] * len(mixed) + [slab] * (2 * len(near)),
            (sheet, whole_table),
        )
        partial = call(
            functools.partial(far_kernel, offsets=far, size=sp),
            (sp_at,),
            (table, partial, *[half for off in far for half in chunks[off]]),
            partial_sum,
            grid,
            [whole_table, sheet] + [slab] * (2 * len(far)),
            sheet,
        )
        projected, squares = call(
            functools.partial(last_kernel, size=sp),
            (sp_at,),
            (table, partial, *chunks[last]),
            (jax.ShapeDtypeStruct((rows, out_cols), bf16), jax.ShapeDtypeStruct((1, rows), f32)),
            grid,
            [
                pl.BlockSpec((1, rows, cols), lambda n, at: (ring_at((place_of(at[0], sp) + last) % sp, sp), 0, 0)),
                sheet,
                slab,
                slab,
            ],
            (sheet, pl.BlockSpec((1, rows), lambda n, at: (0, 0))),
            [pltpu.VMEM((rows, 128), f32)],
        )
    else:
        stacked = jnp.stack(mixed)
        index = jnp.arange(2 * tp, dtype=jnp.int32)
        where = ((index // 2) ^ tp_at[0]) * 2 + (index + odd[0]) % 2
        all_heads = jnp.moveaxis(stacked[where], 0, 1).reshape(rows, width)
        projected = jnp.dot(all_heads, whole_weight, preferred_element_type=f32).astype(bf16)
        branch = lax.optimization_barrier(projected).astype(f32)
        squares = jnp.sum(branch * branch, axis=1)[None]
    squares = lax.psum(squares, "tp")
    sheet = pl.BlockSpec((rows, tile), lambda n, at: (0, n))
    return call(
        functools.partial(norm_kernel, width=width),
        (tp_at,),
        (squares, projected, residual, branch_norm_gain.reshape(1, -1)),
        jax.ShapeDtypeStruct((rows, out_cols), bf16),
        grid,
        [
            pl.BlockSpec((1, rows), lambda n, at: (0, 0)),
            sheet,
            sheet,
            pl.BlockSpec((1, tile), lambda n, at: (0, at[0] * (out_cols // tile) + n)),
        ],
        sheet,
    )


def solution(mesh):
    placed = (
        P("sp", "tp"),
        P("sp", "tp"),
        P("sp", "tp"),
        P("sp", "tp"),
        P(),
        P("tp", "sp"),
        P(),
        P("sp", "tp"),
        P(),
        P("sp", "tp"),
    )
    return jax.shard_map(layer, mesh=mesh, in_specs=placed, out_specs=P("sp", "tp"), check_vma=False)
```

time: 350 us -> 135 us (0.39)
  waiting for transfers between devices: 197 us -> 37.4 us
  Pallas kernels: 0 us -> 52.5 us
  matrix products: 42.7 us -> 0 us
  starting transfers between devices: 0.09 us -> 34.8 us
  blocking collectives: 39 us -> 6.22 us
  other arithmetic: 29.2 us -> 0 us
  local copies, waits for them, and re-layouts: 26.9 us -> 2.9 us
  between operations: 13.3 us -> 0.24 us
    all_gather x3 -> x0, waiting for transfers between devices: 196 us -> none  [the longest x1 127 us: per_device(): whole_weight = lax.all_gather(output_matrix, 'sp', axis=0, tiled=True)]
    pallas_call x0 -> x13, Pallas kernels: none -> 52.5 us  [the longest x10 47.2 us: call(): pl.pallas_call(kernel, grid_spec=spec, out_shape=out_shape)]
    dot_general x34 -> x0, matrix products: 42.7 us -> none  [the longest x8 9.24 us: block_update(): jnp.einsum('hsd,hse->hde', keys_in * jnp.exp(ending - running), values_in...]
    ppermute x0 -> x24, waiting for transfers between devices: none -> 37.4 us  [permute(): return lax.ppermute(array, axis, pairs)]
    ppermute x0 -> x24, starting transfers between devices: none -> 34.8 us  [permute(): return lax.ppermute(array, axis, pairs)]
    all_gather x1 -> x0, blocking collectives: 33.1 us -> none  [prefix(): everything = jax.tree.map(lambda part: lax.all_gather(part, axis), shard)]
    dynamic_slice x26 -> x0, local copies, waits for them, and re-layouts: 17.5 us -> none  [the longest x24 17.5 us: per_device(): lax.scan(step_forward, starting_state, (queries, to_blocks(keys_in), to_b...]
    select_n x8 -> x0, other arithmetic: 11 us -> none  [step(): return jax.tree.map(lambda a, b: jnp.where(reached, a, b), new, before)]
  transfers between devices with their start and end apart: 3 -> 24, of which waited for: 3 -> 10; matrix products, arithmetic and copies ran while one was open for 2% -> 0% of each run, Pallas kernels for 0% -> 27%
where the time goes in v1:
time: 135 us; the launch traced here: 134 us
  Pallas kernels  52.5 us (39%)
  waiting for transfers between devices  37.4 us (28%)
  starting transfers between devices  34.8 us (26%)
  blocking collectives  6.22 us (5%)
  local copies, waits for them, and re-layouts  2.9 us (2%)
    pallas_call x10, Pallas kernels, call(): pl.pallas_call(kernel, grid_spec=spec, out_shape=out_shape)  47.2 us
    ppermute x24, waiting for transfers between devices, permute(): return lax.ppermute(array, axis, pairs)  37.4 us
    ppermute x24, starting transfers between devices, permute(): return lax.ppermute(array, axis, pairs)  34.8 us
    psum x1, blocking collectives, layer(): squares = lax.psum(squares, 'tp')  6.22 us
    unnamed x38, local copies, waits for them, and re-layouts  2.83 us
  transfers between devices with their start and end apart: 24, of which 10 were waited for; matrix products, arithmetic and copies ran while one was open for 0% of the time, Pallas kernels for 27%

profile of v1, /device:TPU:0, one launch (start us, length us, event | category | flops | bytes accessed | tf_op | source)
XLA Modules:
  0.0 134.1 jit_solution(11523812145690281326)
XLA Ops:
  0.0 3.9 %shard_map.102 = (f32[512,512]{1,0:T(8,128)}, bf16[4,136,128]{2,1,0:T(8,128)(2,1)}) custom-call(s32[1]{0:T(128)S(6)} %mul.7.first_ref, s32[1]{0:T(128)} %bitcast.tp_ref, bf16[512,1024]{1,0:T(8,128)(2,1)} %forget_ref.7, bf16[512,1024]{1,0:T(8,128)(2,1)} %value_ref.7, f32[8,512]{1,0:T(8,128)} %surge_ref.3, f32[32,1,128]{2,1,0:T(1,128)} %bitcast.5), custom_call_target="tpu_custom_call" | custom-call | tf_op jit(solution)/shard_map/pallas_call | solution.py:259
  3.9 3.0 %collective-permute-start = (bf16[4,136,128]{2,1,0:T(8,128)(2,1)}, bf16[4,136,128]{2,1,0:T(8,128)(2,1)S(1)}, u32[]{:S(2)}, u32[]{:S(2)}) collective-permute-start(bf16[4,136,128]{2,1,0:T(8,128)(2,1)} %get-tuple-element.23), channel_id=1, source_target_pairs={{0,4},{4,0},{8,12},{12,8},{16,20},{20,16},{24,28},{28,24},{1,5},{5... | collective-permute-start | bytes 417800 | tf_op jit(solution)/shard_map/ppermute | solution.py:263
  6.9 3.7 %shard_map.100 = (f32[512,512]{1,0:T(8,128)}, bf16[4,136,128]{2,1,0:T(8,128)(2,1)}) custom-call(s32[1]{0:T(128)S(6)} %mul.6.first_ref, s32[1]{0:T(128)} %bitcast.tp_ref, bf16[512,1024]{1,0:T(8,128)(2,1)} %forget_ref.7, bf16[512,1024]{1,0:T(8,128)(2,1)} %value_ref.7, f32[8,512]{1,0:T(8,128)} %surge_ref.3, f32[32,1,128]{2,1,0:T(1,128)} %bitcast.6), custom_call_target="tpu_custom_call" | custom-call | tf_op jit(solution)/shard_map/pallas_call | solution.py:259
  11.4 1.7 %pair.1.later_ref = bf16[4,136,128]{2,1,0:T(8,128)(2,1)} custom-call(s32[1]{0:T(128)S(6)} %select_n.7.odd_ref, bf16[4,136,128]{2,1,0:T(8,128)(2,1)} %get-tuple-element.22.own_ref, bf16[4,136,128]{2,1,0:T(8,128)(2,1)} %copy-done.3), custom_call_target="tpu_custom_call" | custom-call | tf_op jit(solution)/shard_map/pair/pallas_call | solution.py:301
  13.1 3.7 %collective-permute-start.1 = (bf16[4,136,128]{2,1,0:T(8,128)(2,1)}, bf16[4,136,128]{2,1,0:T(8,128)(2,1)S(1)}, u32[]{:S(2)}, u32[]{:S(2)}) collective-permute-start(bf16[4,136,128]{2,1,0:T(8,128)(2,1)} %pair.1.later_ref), channel_id=1, source_target_pairs={{0,8},{4,12},{8,16},{12,20},{16,24},{20,28},{1,9},{5,13},{9,17},{1... | collective-permute-start | bytes 417800 | tf_op jit(solution)/shard_map/ppermute | solution.py:263
  16.8 2.9 %collective-permute-done.1.earlier_ref.later_ref = bf16[4,136,128]{2,1,0:T(8,128)(2,1)S(1)} collective-permute-done((bf16[4,136,128]{2,1,0:T(8,128)(2,1)}, bf16[4,136,128]{2,1,0:T(8,128)(2,1)S(1)}, u32[]{:S(2)}, u32[]{:S(2)}) %collective-permute-start.1) | collective-permute-done | bytes 139296 | tf_op jit(solution)/shard_map/ppermute | solution.py:263
  20.4 1.7 %combine.1 = bf16[4,136,128]{2,1,0:T(8,128)(2,1)} custom-call(bf16[4,136,128]{2,1,0:T(8,128)(2,1)} %copy-done.4, bf16[4,136,128]{2,1,0:T(8,128)(2,1)} %pair.1.later_ref), custom_call_target="tpu_custom_call" | custom-call | tf_op jit(solution)/shard_map/combine/pallas_call | solution.py:304
  22.1 5.3 %collective-permute-start.2 = (bf16[4,136,128]{2,1,0:T(8,128)(2,1)}, bf16[4,136,128]{2,1,0:T(8,128)(2,1)S(1)}, u32[]{:S(2)}, u32[]{:S(2)}) collective-permute-start(bf16[4,136,128]{2,1,0:T(8,128)(2,1)} %combine.1), channel_id=1, source_target_pairs={{0,16},{4,20},{8,24},{12,28},{1,17},{5,21},{9,25},{13,29},{2,18},{... | collective-permute-start | bytes 417800 | tf_op jit(solution)/shard_map/ppermute | solution.py:263
  27.4 1.6 %collective-permute-start.10 = (bf16[256,1024]{1,0:T(8,128)(2,1)S(1)}, bf16[256,1024]{1,0:T(8,128)(2,1)S(1)}, u32[]{:S(2)}, u32[]{:S(2)}) collective-permute-start(bf16[256,1024]{1,0:T(8,128)(2,1)S(1)} %get-tuple-element.34.refs_8_), channel_id=1, source_target_pairs={{0,8},{8,16},{16,24},{24,28},{28,20},{20,12},{12,4},{4,0},{1,9},{9... | collective-permute-start | bytes 1572872 | tf_op jit(solution)/shard_map/ppermute | solution.py:263
  29.5 1.6 %collective-permute-start.11 = (bf16[256,1024]{1,0:T(8,128)(2,1)S(1)}, bf16[256,1024]{1,0:T(8,128)(2,1)S(1)}, u32[]{:S(2)}, u32[]{:S(2)}) collective-permute-start(bf16[256,1024]{1,0:T(8,128)(2,1)S(1)} %get-tuple-element.33.refs_9_), channel_id=1, source_target_pairs={{0,8},{8,16},{16,24},{24,28},{28,20},{20,12},{12,4},{4,0},{1,9},{9... | collective-permute-start | bytes 1572872 | tf_op jit(solution)/shard_map/ppermute | solution.py:263
  31.5 4.3 %shard_map.101 = (f32[512,512]{1,0:T(8,128)}, bf16[512,512]{1,0:T(8,128)(2,1)}) custom-call(s32[1]{0:T(128)S(6)} %mul.6.first_ref, s32[1]{0:T(128)} %bitcast.tp_ref, bf16[512,1024]{1,0:T(8,128)(2,1)} %query_ref.3, bf16[512,1024]{1,0:T(8,128)(2,1)} %forget_ref.7, bf16[512,1024]{1,0:T(8,128)(2,1)} %value_ref.7, f32[512,512]{1,0:T(8,128)} %get-tuple-element.19.running_ref, ...), custom_call_target="tpu_custom_call" | custom-call | tf_op jit(solution)/shard_map/pallas_call | solution.py:259
  36.6 1.9 %carry.1 = (bf16[4,128,128]{2,1,0:T(8,128)(2,1)}, bf16[4,128,128]{2,1,0:T(8,128)(2,1)}) custom-call(s32[1]{0:T(128)S(6)} %select_n.7.odd_ref, bf16[4,136,128]{2,1,0:T(8,128)(2,1)} %copy-done.16, bf16[4,136,128]{2,1,0:T(8,128)(2,1)} %copy-done.4, bf16[4,136,128]{2,1,0:T(8,128)(2,1)} %get-tuple-element.22.own_ref, bf16[4,136,128]{2,1,0:T(8,128)(2,1)} %copy-done.3), custom_call_target="tpu_custom_call" | custom-call | tf_op jit(solution)/shard_map/carry/pallas_call | solution.py:313
  38.5 2.9 %shard_map.103.refs_0_ = bf16[512,512]{1,0:T(8,128)(2,1)} custom-call(s32[1]{0:T(128)S(6)} %mul.6.first_ref, f32[512,512]{1,0:T(8,128)} %get-tuple-element.20.local_ref, bf16[512,512]{1,0:T(8,128)(2,1)} %get-tuple-element.21.reach_ref, bf16[4,128,128]{2,1,0:T(8,128)(2,1)} %get-tuple-element.24.carried_ref, bf16[512,1024]{1,0:T(8,128)(2,1)} %gate_ref.3, ...), custom_call_target="tpu_custom_call" | custom-call | tf_op jit(solution)/shard_map/pallas_call | solution.py:259
  42.9 1.6 %collective-permute-start.3 = (bf16[4,128,128]{2,1,0:T(8,128)(2,1)S(1)}, bf16[4,128,128]{2,1,0:T(8,128)(2,1)S(1)}, u32[]{:S(2)}, u32[]{:S(2)}) collective-permute-start(bf16[4,128,128]{2,1,0:T(8,128)(2,1)S(1)} %copy-done.18), channel_id=1, source_target_pairs={{0,4},{4,0},{8,12},{12,8},{16,20},{20,16},{24,28},{28,24},{1,5},{5... | collective-permute-start | bytes 393224 | tf_op jit(solution)/shard_map/ppermute | solution.py:263
  44.5 7.2 %collective-permute-done.11.refs_11_ = bf16[256,1024]{1,0:T(8,128)(2,1)S(1)} collective-permute-done((bf16[256,1024]{1,0:T(8,128)(2,1)S(1)}, bf16[256,1024]{1,0:T(8,128)(2,1)S(1)}, u32[]{:S(2)}, u32[]{:S(2)}) %collective-permute-start.11) | collective-permute-done | bytes 524320 | tf_op jit(solution)/shard_map/ppermute | solution.py:263
  51.7 3.9 %collective-permute-start.14 = (bf16[256,1024]{1,0:T(8,128)(2,1)S(1)}, bf16[256,1024]{1,0:T(8,128)(2,1)S(1)}, u32[]{:S(2)}, u32[]{:S(2)}) collective-permute-start(bf16[256,1024]{1,0:T(8,128)(2,1)S(1)} %collective-permute-done.10.refs_10_), channel_id=1, source_target_pairs={{0,8},{8,16},{16,24},{24,28},{28,20},{20,12},{12,4},{4,0},{1,9},{9... | collective-permute-start | bytes 1572872 | tf_op jit(solution)/shard_map/ppermute | solution.py:263
  55.6 2.5 %collective-permute-start.15 = (bf16[256,1024]{1,0:T(8,128)(2,1)S(1)}, bf16[256,1024]{1,0:T(8,128)(2,1)S(1)}, u32[]{:S(2)}, u32[]{:S(2)}) collective-permute-start(bf16[256,1024]{1,0:T(8,128)(2,1)S(1)} %collective-permute-done.11.refs_11_), channel_id=1, source_target_pairs={{0,8},{8,16},{16,24},{24,28},{28,20},{20,12},{12,4},{4,0},{1,9},{9... | collective-permute-start | bytes 1572872 | tf_op jit(solution)/shard_map/ppermute | solution.py:263
  58.2 4.3 %shard_map.104 = (f32[512,512]{1,0:T(8,128)}, bf16[512,512]{1,0:T(8,128)(2,1)}) custom-call(s32[1]{0:T(128)S(6)} %mul.7.first_ref, s32[1]{0:T(128)} %bitcast.tp_ref, bf16[512,1024]{1,0:T(8,128)(2,1)} %query_ref.3, bf16[512,1024]{1,0:T(8,128)(2,1)} %forget_ref.7, bf16[512,1024]{1,0:T(8,128)(2,1)} %value_ref.7, f32[512,512]{1,0:T(8,128)} %get-tuple-element.25.running_ref, ...), custom_call_target="tpu_custom_call" | custom-call | tf_op jit(solution)/shard_map/pallas_call | solution.py:259
  62.6 2.9 %shard_map.105.refs_1_ = bf16[512,512]{1,0:T(8,128)(2,1)} custom-call(s32[1]{0:T(128)S(6)} %mul.7.first_ref, f32[512,512]{1,0:T(8,128)} %get-tuple-element.26.local_ref, bf16[512,512]{1,0:T(8,128)(2,1)} %get-tuple-element.27.reach_ref, bf16[4,128,128]{2,1,0:T(8,128)(2,1)} %copy-done.17, bf16[512,1024]{1,0:T(8,128)(2,1)} %gate_ref.3, f32[1,128]{1,0:T(1,128)} %bitcast.11), custom_call_target="tpu_custom_call" | custom-call | tf_op jit(solution)/shard_map/pallas_call | solution.py:259
  68.0 10.7 %collective-permute-done.15.refs_15_ = bf16[256,1024]{1,0:T(8,128)(2,1)S(1)} collective-permute-done((bf16[256,1024]{1,0:T(8,128)(2,1)S(1)}, bf16[256,1024]{1,0:T(8,128)(2,1)S(1)}, u32[]{:S(2)}, u32[]{:S(2)}) %collective-permute-start.15) | collective-permute-done | bytes 524320 | tf_op jit(solution)/shard_map/ppermute | solution.py:263
  78.7 2.5 %collective-permute-start.18 = (bf16[256,1024]{1,0:T(8,128)(2,1)S(1)}, bf16[256,1024]{1,0:T(8,128)(2,1)}, u32[]{:S(2)}, u32[]{:S(2)}) collective-permute-start(bf16[256,1024]{1,0:T(8,128)(2,1)S(1)} %collective-permute-done.14.refs_14_), channel_id=1, source_target_pairs={{0,8},{8,16},{16,24},{24,28},{28,20},{20,12},{12,4},{4,0},{1,9},{9... | collective-permute-start | bytes 1572872 | tf_op jit(solution)/shard_map/ppermute | solution.py:263
  81.2 2.0 %collective-permute-done.17.refs_17_ = bf16[256,1024]{1,0:T(8,128)(2,1)} collective-permute-done((bf16[256,1024]{1,0:T(8,128)(2,1)S(1)}, bf16[256,1024]{1,0:T(8,128)(2,1)}, u32[]{:S(2)}, u32[]{:S(2)}) %collective-permute-start.17) | collective-permute-done | bytes 524320 | tf_op jit(solution)/shard_map/ppermute | solution.py:263
  83.5 1.8 %collective-permute-start.19 = (bf16[256,1024]{1,0:T(8,128)(2,1)S(1)}, bf16[256,1024]{1,0:T(8,128)(2,1)}, u32[]{:S(2)}, u32[]{:S(2)}) collective-permute-start(bf16[256,1024]{1,0:T(8,128)(2,1)S(1)} %collective-permute-done.15.refs_15_), channel_id=1, source_target_pairs={{0,8},{8,16},{16,24},{24,28},{28,20},{20,12},{12,4},{4,0},{1,9},{9... | collective-permute-start | bytes 1572872 | tf_op jit(solution)/shard_map/ppermute | solution.py:263
  85.6 8.0 %collective-permute-done.18.refs_2_ = bf16[256,1024]{1,0:T(8,128)(2,1)} collective-permute-done((bf16[256,1024]{1,0:T(8,128)(2,1)S(1)}, bf16[256,1024]{1,0:T(8,128)(2,1)}, u32[]{:S(2)}, u32[]{:S(2)}) %collective-permute-start.18) | collective-permute-done | bytes 524320 | tf_op jit(solution)/shard_map/ppermute | solution.py:263
  93.6 2.5 %collective-permute-start.22 = (bf16[256,1024]{1,0:T(8,128)(2,1)}, bf16[256,1024]{1,0:T(8,128)(2,1)S(1)}, u32[]{:S(2)}, u32[]{:S(2)}) collective-permute-start(bf16[256,1024]{1,0:T(8,128)(2,1)} %collective-permute-done.18.refs_2_), channel_id=1, source_target_pairs={{0,8},{8,16},{16,24},{24,28},{28,20},{20,12},{12,4},{4,0},{1,9},{9... | collective-permute-start | bytes 1572872 | tf_op jit(solution)/shard_map/ppermute | solution.py:263
  96.1 2.2 %collective-permute-done.21.refs_5_ = bf16[256,1024]{1,0:T(8,128)(2,1)} collective-permute-done((bf16[256,1024]{1,0:T(8,128)(2,1)}, bf16[256,1024]{1,0:T(8,128)(2,1)}, u32[]{:S(2)}, u32[]{:S(2)}) %collective-permute-start.21) | collective-permute-done | bytes 524320 | tf_op jit(solution)/shard_map/ppermute | solution.py:263
  99.5 9.5 %shard_map.106 = (f32[512,1024]{1,0:T(8,128)}, bf16[8,512,512]{2,1,0:T(8,128)(2,1)}) custom-call(s32[1]{0:T(128)} %bitcast.1.sp_ref, s32[1]{0:T(128)} %bitcast.tp_ref, bf16[512,512]{1,0:T(8,128)(2,1)} %shard_map.103.refs_0_, bf16[512,512]{1,0:T(8,128)(2,1)} %shard_map.105.refs_1_, bf16[512,512]{1,0:T(8,128)(2,1)} %collective-permute-done.4.refs_2_, ...), custom_call_target="tpu_custom_call" | custom-call | tf_op jit(solution)/shard_map/pallas_call | solution.py:259
  109.5 6.6 %shard_map.107.partial_ref = f32[512,1024]{1,0:T(8,128)} custom-call(s32[1]{0:T(128)} %bitcast.1.sp_ref, bf16[8,512,512]{2,1,0:T(8,128)(2,1)} %get-tuple-element.29.refs_0_.table, f32[512,1024]{1,0:T(8,128)} %get-tuple-element.30.refs_1_, bf16[256,1024]{1,0:T(8,128)(2,1)} %collective-permute-done.18.refs_2_, ...), custom_call_target="tpu_custom_call" | custom-call | tf_op jit(solution)/shard_map/pallas_call | solution.py:259
  116.1 2.7 %collective-permute-done.23.second_ref = bf16[256,1024]{1,0:T(8,128)(2,1)} collective-permute-done((bf16[256,1024]{1,0:T(8,128)(2,1)}, bf16[256,1024]{1,0:T(8,128)(2,1)}, u32[]{:S(2)}, u32[]{:S(2)}) %collective-permute-start.23) | collective-permute-done | bytes 524320 | tf_op jit(solution)/shard_map/ppermute | solution.py:263
  118.8 5.0 %shard_map.108 = (bf16[512,1024]{1,0:T(8,128)(2,1)}, f32[1,512]{1,0:T(1,128)}) custom-call(s32[1]{0:T(128)} %bitcast.1.sp_ref, bf16[8,512,512]{2,1,0:T(8,128)(2,1)} %get-tuple-element.29.refs_0_.table, f32[512,1024]{1,0:T(8,128)} %shard_map.107.partial_ref, bf16[256,1024]{1,0:T(8,128)(2,1)} %copy-done.15, bf16[256,1024]{1,0:T(8,128)(2,1)} %collective-permute-done.23.second_ref), custom_call_target="tpu_custom_call" | custom-call | tf_op jit(solution)/shard_map/pallas_call | solution.py:259
  123.8 6.2 %psum.7.square_ref = f32[1,512]{1,0:T(1,128)} all-reduce(f32[1,512]{1,0:T(1,128)} %get-tuple-element.31), channel_id=1, replica_groups=mesh['sp'=8,'tp'=4] {'tp'}, use_global_device_ids=true, to_apply=%region_0.1 | all-reduce | flops 512 | bytes 4096 | tf_op jit(solution)/shard_map/psum | solution.py:469
  130.0 4.1 %shard_map.109 = bf16[512,1024]{1,0:T(8,128)(2,1)} custom-call(s32[1]{0:T(128)} %bitcast.tp_ref, f32[1,512]{1,0:T(1,128)} %psum.7.square_ref, bf16[512,1024]{1,0:T(8,128)(2,1)} %get-tuple-element.32.projected_ref, bf16[512,1024]{1,0:T(8,128)(2,1)} %residual_ref.1, f32[1,4096]{1,0:T(1,128)} %bitcast.9), custom_call_target="tpu_custom_call" | custom-call | tf_op jit(solution)/shard_map/pallas_call | solution.py:259
  (69 shorter events, 9.5 us)
Async XLA Ops:
  0.0 27.3 %copy-start.2 = (bf16[512,1024]{1,0:T(8,128)(2,1)S(1)}, bf16[512,1024]{1,0:T(8,128)(2,1)}, u32[]{:S(2)}) copy-start(bf16[512,1024]{1,0:T(8,128)(2,1)} %param.17) | copy-start | bytes 3145732
  3.9 6.8 %collective-permute-start = (bf16[4,136,128]{2,1,0:T(8,128)(2,1)}, bf16[4,136,128]{2,1,0:T(8,128)(2,1)S(1)}, u32[]{:S(2)}, u32[]{:S(2)}) collective-permute-start(bf16[4,136,128]{2,1,0:T(8,128)(2,1)} %get-tuple-element.23), channel_id=1, source_target_pairs={{0,4},{4,0},{8,12},{12,8},{16,20},{20,16},{24,28},{28,24},{1,5},{5... | collective-permute-start | bytes 417800 | tf_op jit(solution)/shard_map/ppermute | solution.py:263
  13.1 6.6 %collective-permute-start.1 = (bf16[4,136,128]{2,1,0:T(8,128)(2,1)}, bf16[4,136,128]{2,1,0:T(8,128)(2,1)S(1)}, u32[]{:S(2)}, u32[]{:S(2)}) collective-permute-start(bf16[4,136,128]{2,1,0:T(8,128)(2,1)} %pair.1.later_ref), channel_id=1, source_target_pairs={{0,8},{4,12},{8,16},{12,20},{16,24},{20,28},{1,9},{5,13},{9,17},{1... | collective-permute-start | bytes 417800 | tf_op jit(solution)/shard_map/ppermute | solution.py:263
  22.1 13.8 %collective-permute-start.2 = (bf16[4,136,128]{2,1,0:T(8,128)(2,1)}, bf16[4,136,128]{2,1,0:T(8,128)(2,1)S(1)}, u32[]{:S(2)}, u32[]{:S(2)}) collective-permute-start(bf16[4,136,128]{2,1,0:T(8,128)(2,1)} %combine.1), channel_id=1, source_target_pairs={{0,16},{4,20},{8,24},{12,28},{1,17},{5,21},{9,25},{13,29},{2,18},{... | collective-permute-start | bytes 417800 | tf_op jit(solution)/shard_map/ppermute | solution.py:263
  27.4 15.5 %collective-permute-start.10 = (bf16[256,1024]{1,0:T(8,128)(2,1)S(1)}, bf16[256,1024]{1,0:T(8,128)(2,1)S(1)}, u32[]{:S(2)}, u32[]{:S(2)}) collective-permute-start(bf16[256,1024]{1,0:T(8,128)(2,1)S(1)} %get-tuple-element.34.refs_8_), channel_id=1, source_target_pairs={{0,8},{8,16},{16,24},{24,28},{28,20},{20,12},{12,4},{4,0},{1,9},{9... | collective-permute-start | bytes 1572872 | tf_op jit(solution)/shard_map/ppermute | solution.py:263
  29.1 22.6 %collective-permute-start.12 = (bf16[256,1024]{1,0:T(8,128)(2,1)S(1)}, bf16[256,1024]{1,0:T(8,128)(2,1)S(1)}, u32[]{:S(2)}, u32[]{:S(2)}) collective-permute-start(bf16[256,1024]{1,0:T(8,128)(2,1)S(1)} %get-tuple-element.34.refs_8_), channel_id=1, source_target_pairs={{8,0},{16,8},{24,16},{28,24},{20,28},{12,20},{4,12},{0,4},{9,1},{1... | collective-permute-start | bytes 1572872 | tf_op jit(solution)/shard_map/ppermute | solution.py:263
  29.5 22.2 %collective-permute-start.11 = (bf16[256,1024]{1,0:T(8,128)(2,1)S(1)}, bf16[256,1024]{1,0:T(8,128)(2,1)S(1)}, u32[]{:S(2)}, u32[]{:S(2)}) collective-permute-start(bf16[256,1024]{1,0:T(8,128)(2,1)S(1)} %get-tuple-element.33.refs_9_), channel_id=1, source_target_pairs={{0,8},{8,16},{16,24},{24,28},{28,20},{20,12},{12,4},{4,0},{1,9},{9... | collective-permute-start | bytes 1572872 | tf_op jit(solution)/shard_map/ppermute | solution.py:263
  31.1 24.6 %collective-permute-start.13 = (bf16[256,1024]{1,0:T(8,128)(2,1)S(1)}, bf16[256,1024]{1,0:T(8,128)(2,1)S(1)}, u32[]{:S(2)}, u32[]{:S(2)}) collective-permute-start(bf16[256,1024]{1,0:T(8,128)(2,1)S(1)} %get-tuple-element.33.refs_9_), channel_id=1, source_target_pairs={{8,0},{16,8},{24,16},{28,24},{20,28},{12,20},{4,12},{0,4},{9,1},{1... | collective-permute-start | bytes 1572872 | tf_op jit(solution)/shard_map/ppermute | solution.py:263
  41.4 16.7 %collective-permute-start.6 = (bf16[512,512]{1,0:T(8,128)(2,1)}, bf16[512,512]{1,0:T(8,128)(2,1)}, u32[]{:S(2)}, u32[]{:S(2)}) collective-permute-start(bf16[512,512]{1,0:T(8,128)(2,1)} %shard_map.103.refs_0_), channel_id=1, source_target_pairs={{0,2},{1,3},{2,0},{3,1},{4,6},{5,7},{6,4},{7,5},{8,10},{9,11},{10,... | collective-permute-start | bytes 1572872 | tf_op jit(solution)/shard_map/ppermute | solution.py:263
  42.9 19.6 %copy-start.5 = (bf16[256,1024]{1,0:T(8,128)(2,1)}, bf16[256,1024]{1,0:T(8,128)(2,1)S(1)}, u32[]{:S(2)}) copy-start(bf16[256,1024]{1,0:T(8,128)(2,1)S(1)} %collective-permute-done.10.refs_10_) | copy-start | bytes 1572868
  42.9 15.2 %collective-permute-start.3 = (bf16[4,128,128]{2,1,0:T(8,128)(2,1)S(1)}, bf16[4,128,128]{2,1,0:T(8,128)(2,1)S(1)}, u32[]{:S(2)}, u32[]{:S(2)}) collective-permute-start(bf16[4,128,128]{2,1,0:T(8,128)(2,1)S(1)} %copy-done.18), channel_id=1, source_target_pairs={{0,4},{4,0},{8,12},{12,8},{16,20},{20,16},{24,28},{28,24},{1,5},{5... | collective-permute-start | bytes 393224 | tf_op jit(solution)/shard_map/ppermute | solution.py:263
  51.7 10.9 %copy-start.7 = (bf16[256,1024]{1,0:T(8,128)(2,1)}, bf16[256,1024]{1,0:T(8,128)(2,1)S(1)}, u32[]{:S(2)}) copy-start(bf16[256,1024]{1,0:T(8,128)(2,1)S(1)} %collective-permute-done.11.refs_11_) | copy-start | bytes 1572868
  51.7 13.8 %collective-permute-start.4 = (bf16[512,512]{1,0:T(8,128)(2,1)}, bf16[512,512]{1,0:T(8,128)(2,1)}, u32[]{:S(2)}, u32[]{:S(2)}) collective-permute-start(bf16[512,512]{1,0:T(8,128)(2,1)} %shard_map.103.refs_0_), channel_id=1, source_target_pairs={{0,1},{1,0},{2,3},{3,2},{4,5},{5,4},{6,7},{7,6},{8,9},{9,8},{10,11... | collective-permute-start | bytes 1572872 | tf_op jit(solution)/shard_map/ppermute | solution.py:263
  51.7 10.9 %copy-start.6 = (bf16[256,1024]{1,0:T(8,128)(2,1)}, bf16[256,1024]{1,0:T(8,128)(2,1)S(1)}, u32[]{:S(2)}) copy-start(bf16[256,1024]{1,0:T(8,128)(2,1)S(1)} %collective-permute-done.12.refs_12_) | copy-start | bytes 1572868
  51.7 16.3 %collective-permute-start.14 = (bf16[256,1024]{1,0:T(8,128)(2,1)S(1)}, bf16[256,1024]{1,0:T(8,128)(2,1)S(1)}, u32[]{:S(2)}, u32[]{:S(2)}) collective-permute-start(bf16[256,1024]{1,0:T(8,128)(2,1)S(1)} %collective-permute-done.10.refs_10_), channel_id=1, source_target_pairs={{0,8},{8,16},{16,24},{24,28},{28,20},{20,12},{12,4},{4,0},{1,9},{9... | collective-permute-start | bytes 1572872 | tf_op jit(solution)/shard_map/ppermute | solution.py:263
  55.6 23.0 %collective-permute-start.15 = (bf16[256,1024]{1,0:T(8,128)(2,1)S(1)}, bf16[256,1024]{1,0:T(8,128)(2,1)S(1)}, u32[]{:S(2)}, u32[]{:S(2)}) collective-permute-start(bf16[256,1024]{1,0:T(8,128)(2,1)S(1)} %collective-permute-done.11.refs_11_), channel_id=1, source_target_pairs={{0,8},{8,16},{16,24},{24,28},{28,20},{20,12},{12,4},{4,0},{1,9},{9... | collective-permute-start | bytes 1572872 | tf_op jit(solution)/shard_map/ppermute | solution.py:263
  58.1 20.5 %collective-permute-start.16 = (bf16[256,1024]{1,0:T(8,128)(2,1)S(1)}, bf16[256,1024]{1,0:T(8,128)(2,1)}, u32[]{:S(2)}, u32[]{:S(2)}) collective-permute-start(bf16[256,1024]{1,0:T(8,128)(2,1)S(1)} %collective-permute-done.12.refs_12_), channel_id=1, source_target_pairs={{8,0},{16,8},{24,16},{28,24},{20,28},{12,20},{4,12},{0,4},{9,1},{1... | collective-permute-start | bytes 1572872 | tf_op jit(solution)/shard_map/ppermute | solution.py:263
  58.2 25.0 %collective-permute-start.17 = (bf16[256,1024]{1,0:T(8,128)(2,1)S(1)}, bf16[256,1024]{1,0:T(8,128)(2,1)}, u32[]{:S(2)}, u32[]{:S(2)}) collective-permute-start(bf16[256,1024]{1,0:T(8,128)(2,1)S(1)} %collective-permute-done.13.refs_13_), channel_id=1, source_target_pairs={{8,0},{16,8},{24,16},{28,24},{20,28},{12,20},{4,12},{0,4},{9,1},{1... | collective-permute-start | bytes 1572872 | tf_op jit(solution)/shard_map/ppermute | solution.py:263
  65.5 18.0 %collective-permute-start.7 = (bf16[512,512]{1,0:T(8,128)(2,1)}, bf16[512,512]{1,0:T(8,128)(2,1)S(1)}, u32[]{:S(2)}, u32[]{:S(2)}) collective-permute-start(bf16[512,512]{1,0:T(8,128)(2,1)} %shard_map.105.refs_1_), channel_id=1, source_target_pairs={{0,2},{1,3},{2,0},{3,1},{4,6},{5,7},{6,4},{7,5},{8,10},{9,11},{10,... | collective-permute-start | bytes 1572872 | tf_op jit(solution)/shard_map/ppermute | solution.py:263
  68.0 30.6 %copy-start.9 = (bf16[256,1024]{1,0:T(8,128)(2,1)}, bf16[256,1024]{1,0:T(8,128)(2,1)S(1)}, u32[]{:S(2)}) copy-start(bf16[256,1024]{1,0:T(8,128)(2,1)S(1)} %collective-permute-done.14.refs_14_) | copy-start | bytes 1572868
  68.0 15.5 %collective-permute-start.5 = (bf16[512,512]{1,0:T(8,128)(2,1)}, bf16[512,512]{1,0:T(8,128)(2,1)S(1)}, u32[]{:S(2)}, u32[]{:S(2)}) collective-permute-start(bf16[512,512]{1,0:T(8,128)(2,1)} %shard_map.105.refs_1_), channel_id=1, source_target_pairs={{0,1},{1,0},{2,3},{3,2},{4,5},{5,4},{6,7},{7,6},{8,9},{9,8},{10,11... | collective-permute-start | bytes 1572872 | tf_op jit(solution)/shard_map/ppermute | solution.py:263
  78.7 19.9 %copy-start.10 = (bf16[256,1024]{1,0:T(8,128)(2,1)}, bf16[256,1024]{1,0:T(8,128)(2,1)S(1)}, u32[]{:S(2)}) copy-start(bf16[256,1024]{1,0:T(8,128)(2,1)S(1)} %collective-permute-done.15.refs_15_) | copy-start | bytes 1572868
  78.7 6.6 %collective-permute-start.8 = (bf16[512,512]{1,0:T(8,128)(2,1)}, bf16[512,512]{1,0:T(8,128)(2,1)S(1)}, u32[]{:S(2)}, u32[]{:S(2)}) collective-permute-start(bf16[512,512]{1,0:T(8,128)(2,1)} %collective-permute-done.6.refs_4_), channel_id=1, source_target_pairs={{0,1},{1,0},{2,3},{3,2},{4,5},{5,4},{6,7},{7,6},{8,9},{9,8},{10,11... | collective-permute-start | bytes 1572872 | tf_op jit(solution)/shard_map/ppermute | solution.py:263
  78.7 14.9 %collective-permute-start.18 = (bf16[256,1024]{1,0:T(8,128)(2,1)S(1)}, bf16[256,1024]{1,0:T(8,128)(2,1)}, u32[]{:S(2)}, u32[]{:S(2)}) collective-permute-start(bf16[256,1024]{1,0:T(8,128)(2,1)S(1)} %collective-permute-done.14.refs_14_), channel_id=1, source_target_pairs={{0,8},{8,16},{16,24},{24,28},{28,20},{20,12},{12,4},{4,0},{1,9},{9... | collective-permute-start | bytes 1572872 | tf_op jit(solution)/shard_map/ppermute | solution.py:263
  83.2 15.1 %collective-permute-start.21 = (bf16[256,1024]{1,0:T(8,128)(2,1)}, bf16[256,1024]{1,0:T(8,128)(2,1)}, u32[]{:S(2)}, u32[]{:S(2)}) collective-permute-start(bf16[256,1024]{1,0:T(8,128)(2,1)} %collective-permute-done.17.refs_17_), channel_id=1, source_target_pairs={{8,0},{16,8},{24,16},{28,24},{20,28},{12,20},{4,12},{0,4},{9,1},{1... | collective-permute-start | bytes 1572872 | tf_op jit(solution)/shard_map/ppermute | solution.py:263
  83.5 15.1 %collective-permute-start.9 = (bf16[512,512]{1,0:T(8,128)(2,1)S(1)}, bf16[512,512]{1,0:T(8,128)(2,1)S(1)}, u32[]{:S(2)}, u32[]{:S(2)}) collective-permute-start(bf16[512,512]{1,0:T(8,128)(2,1)S(1)} %collective-permute-done.7.refs_5_), channel_id=1, source_target_pairs={{0,1},{1,0},{2,3},{3,2},{4,5},{5,4},{6,7},{7,6},{8,9},{9,8},{10,11... | collective-permute-start | bytes 1572872 | tf_op jit(solution)/shard_map/ppermute | solution.py:263
  83.5 15.1 %copy-start.12 = (bf16[512,512]{1,0:T(8,128)(2,1)}, bf16[512,512]{1,0:T(8,128)(2,1)S(1)}, u32[]{:S(2)}) copy-start(bf16[512,512]{1,0:T(8,128)(2,1)S(1)} %collective-permute-done.5.refs_3_) | copy-start | bytes 1572868
  83.5 25.4 %collective-permute-start.19 = (bf16[256,1024]{1,0:T(8,128)(2,1)S(1)}, bf16[256,1024]{1,0:T(8,128)(2,1)}, u32[]{:S(2)}, u32[]{:S(2)}) collective-permute-start(bf16[256,1024]{1,0:T(8,128)(2,1)S(1)} %collective-permute-done.15.refs_15_), channel_id=1, source_target_pairs={{0,8},{8,16},{16,24},{24,28},{28,20},{20,12},{12,4},{4,0},{1,9},{9... | collective-permute-start | bytes 1572872 | tf_op jit(solution)/shard_map/ppermute | solution.py:263
  85.3 13.3 %copy-start.13 = (bf16[512,512]{1,0:T(8,128)(2,1)}, bf16[512,512]{1,0:T(8,128)(2,1)S(1)}, u32[]{:S(2)}) copy-start(bf16[512,512]{1,0:T(8,128)(2,1)S(1)} %collective-permute-done.8.refs_6_) | copy-start | bytes 1572868
  85.3 24.2 %collective-permute-start.20 = (bf16[256,1024]{1,0:T(8,128)(2,1)}, bf16[256,1024]{1,0:T(8,128)(2,1)}, u32[]{:S(2)}, u32[]{:S(2)}) collective-permute-start(bf16[256,1024]{1,0:T(8,128)(2,1)} %collective-permute-done.16.refs_16_), channel_id=1, source_target_pairs={{8,0},{16,8},{24,16},{28,24},{20,28},{12,20},{4,12},{0,4},{9,1},{1... | collective-permute-start | bytes 1572872 | tf_op jit(solution)/shard_map/ppermute | solution.py:263
  93.6 22.5 %collective-permute-start.22 = (bf16[256,1024]{1,0:T(8,128)(2,1)}, bf16[256,1024]{1,0:T(8,128)(2,1)S(1)}, u32[]{:S(2)}, u32[]{:S(2)}) collective-permute-start(bf16[256,1024]{1,0:T(8,128)(2,1)} %collective-permute-done.18.refs_2_), channel_id=1, source_target_pairs={{0,8},{8,16},{16,24},{24,28},{28,20},{20,12},{12,4},{4,0},{1,9},{9... | collective-permute-start | bytes 1572872 | tf_op jit(solution)/shard_map/ppermute | solution.py:263
  98.3 20.5 %collective-permute-start.23 = (bf16[256,1024]{1,0:T(8,128)(2,1)}, bf16[256,1024]{1,0:T(8,128)(2,1)}, u32[]{:S(2)}, u32[]{:S(2)}) collective-permute-start(bf16[256,1024]{1,0:T(8,128)(2,1)} %collective-permute-done.21.refs_5_), channel_id=1, source_target_pairs={{8,0},{16,8},{24,16},{28,24},{20,28},{12,20},{4,12},{0,4},{9,1},{1... | collective-permute-start | bytes 1572872 | tf_op jit(solution)/shard_map/ppermute | solution.py:263
  (11 other events, 48.4 us)

commit v2 on v1

--- a/solution.py
+++ b/solution.py
@@ -12,6 +12,7 @@
 SPAN = 128
 EXTRA = 8
 TILE = 256
+ROOM = pltpu.CompilerParams(vmem_limit_bytes=32 * 2**20)
 epsilon = 1e-06
 
 
@@ -52,7 +53,7 @@
 
 def states_kernel(first_ref, tp_ref, forget_ref, value_ref, surge_ref, gap_ref, running_ref, packed_ref, column_ref):
     step = pl.program_id(0)
-    per = packed_ref.shape[0]
+    per = gap_ref.shape[0]
     rows = forget_ref.shape[0]
 
     @pl.when(step == 0)
@@ -78,8 +79,8 @@
             after = after + running[SPAN - 1 :, :]
             keys.append((gates[part] * jnp.exp(after - running)).astype(bf16))
         keys = jnp.concatenate(keys[::-1], axis=0)
-        packed_ref[i, :HEAD_DIM, :] = dot(value_ref[:, cols], keys, TN).astype(bf16)
-        packed_ref[i, HEAD_DIM:, :] = pack_decay(jnp.exp(after))
+        packed_ref[step * per + i, :HEAD_DIM, :] = dot(value_ref[:, cols], keys, TN).astype(bf16)
+        packed_ref[step * per + i, HEAD_DIM:, :] = pack_decay(jnp.exp(after))
 
 
 def local_kernel(first_ref, tp_ref, query_ref, forget_ref, value_ref, running_ref, gap_ref, local_ref, reach_ref):
@@ -150,9 +151,11 @@
 
 
 def mix_kernel(first_ref, local_ref, reach_ref, carried_ref, gate_ref, gain_ref, out_ref):
-    for i in range(carried_ref.shape[0]):
+    per = out_ref.shape[1] // HEAD_DIM
+    for i in range(per):
         cols = slice(i * HEAD_DIM, (i + 1) * HEAD_DIM)
-        heads_out = local_ref[:, cols] + dot(reach_ref[:, cols], carried_ref[i], NT)
+        carried = carried_ref[pl.program_id(0) * per + i]
+        heads_out = local_ref[:, cols] + dot(reach_ref[:, cols], carried, NT)
         mean_sq = jnp.mean(heads_out * heads_out, axis=1, keepdims=True)
         logits = gate_ref[:, cols].astype(f32)
         gates = logits / (1.0 + jnp.exp(-logits))
@@ -168,69 +171,43 @@
     return jnp.where(member % 2 == 0, member // 2, size - 1 - member // 2)
 
 
-def near_kernel(sp_ref, tp_ref, *refs, offsets, size, n_mixed):
+def project_kernel(sp_ref, tp_ref, *refs, offsets, size, n_mixed):
     mixed = refs[:n_mixed]
-    chunks = refs[n_mixed:-2]
-    out_ref, table = refs[-2:]
+    chunks = refs[n_mixed:-3]
+    out_ref, piece_ref, table = refs[-3:]
     at = place_of(sp_ref[0], size)
-    per = 2
-
-    @pl.when(pl.program_id(0) == 0)
-    def _():
-        for i, piece in enumerate(mixed):
-            group = (i + sp_ref[0]) % 2
-            table[(tp_ref[0] ^ (i // per)) * per + group] = piece[...]
-
-    total = None
     half = chunks[0].shape[0]
-    for i, offset in enumerate(offsets):
-        block = ring_at((at + (offset + size)) % size, size)
-        for j in range(2):
-            part = dot(table[block, :, j * half : (j + 1) * half], chunks[2 * i + j][...])
-            total = part if total is None else total + part
-    out_ref[...] = total
-
-
-def far_kernel(sp_ref, *refs, offsets, size):
-    table, partial_ref = refs[:2]
-    chunks = refs[2:-1]
-    out_ref = refs[-1]
-    at = place_of(sp_ref[0], size)
-    total = partial_ref[...]
-    half = chunks[0].shape[0]
-    for i, offset in enumerate(offsets):
-        block = ring_at((at + (offset + size)) % size, size)
-        for j in range(2):
-            total = total + dot(table[block, :, j * half : (j + 1) * half], chunks[2 * i + j][...])
-    out_ref[...] = total
-
-
-def last_kernel(sp_ref, table, partial_ref, first_ref, second_ref, out_ref, square_ref, lanes_ref, *, size):
-    del sp_ref
+    for i, piece in enumerate(mixed):
+        group = (i + sp_ref[0]) % 2
+        table[(tp_ref[0] ^ (i // 2)) * 2 + group] = piece[...]
+    piece_ref[...] = table[ring_at((at + size // 2) % size, size)]
+    for start in range(0, out_ref.shape[1], TILE):
+        cols = slice(start, start + TILE)
+        total = None
+        for i, offset in enumerate(offsets):
+            block = ring_at((at + (offset + size)) % size, size)
+            for j in range(2):
+                part = dot(table[block, :, j * half : (j + 1) * half], chunks[2 * i + j][:, cols])
+                total = part if total is None else total + part
+        out_ref[:, cols] = total
+
+
+def last_kernel(partial_ref, piece_ref, first_ref, second_ref, out_ref, square_ref, lanes_ref):
     half = first_ref.shape[0]
-    total = partial_ref[...] + dot(table[0, :, :half], first_ref[...])
-    total = total + dot(table[0, :, half:], second_ref[...])
-    rounded = total.astype(bf16)
-    out_ref[...] = rounded
-    wide = rounded.astype(f32)
-    squares = wide * wide
-    lanes = squares[:, :128]
-    for start in range(128, squares.shape[1], 128):
-        lanes = lanes + squares[:, start : start + 128]
-
-    @pl.when(pl.program_id(0) == 0)
-    def _():
-        lanes_ref[...] = lanes
-
-    @pl.when(pl.program_id(0) > 0)
-    def _():
-        lanes_ref[...] += lanes
-
-    @pl.when(pl.program_id(0) == pl.num_programs(0) - 1)
-    def _():
-        high, low = split2(lanes_ref[...])
-        ones = jnp.ones((8, 128), bf16)
-        square_ref[...] = (dot(ones, high, NT) + dot(ones, low, NT))[:1]
+    for start in range(0, out_ref.shape[1], TILE):
+        cols = slice(start, start + TILE)
+        total = partial_ref[:, cols] + dot(piece_ref[:, :half], first_ref[:, cols])
+        rounded = (total + dot(piece_ref[:, half:], second_ref[:, cols])).astype(bf16)
+        out_ref[:, cols] = rounded
+        wide = rounded.astype(f32)
+        squares = wide * wide
+        lanes = squares[:, :128]
+        for first in range(128, TILE, 128):
+            lanes = lanes + squares[:, first : first + 128]
+        lanes_ref[...] = lanes if start == 0 else lanes_ref[...] + lanes
+    high, low = split2(lanes_ref[...])
+    ones = jnp.ones((8, 128), bf16)
+    square_ref[...] = (dot(ones, high, NT) + dot(ones, low, NT))[:1]
 
 
 def norm_kernel(tp_ref, square_ref, projected_ref, residual_ref, gain_ref, out_ref, *, width):
@@ -246,6 +223,21 @@
 
 def smem():
     return pl.BlockSpec(memory_space=pltpu.SMEM)
+
+
+def resident(array):
+    return pltpu.with_memory_space_constraint(array, pltpu.VMEM)
+
+
+def small(kernel, scalars, operands, outs, scratch=()):
+    return pl.pallas_call(
+        kernel,
+        out_shape=tuple(pltpu.VMEM(*out) for out in outs),
+        in_specs=[smem()] * len(scalars) + [vmem()] * len(operands),
+        out_specs=tuple(vmem() for _ in outs),
+        scratch_shapes=list(scratch),
+        compiler_params=ROOM,
+    )(*scalars, *[resident(array) for array in operands])
 
 
 def call(kernel, scalars, operands, out_shape, grid, in_specs, out_specs, scratch=()):
@@ -256,7 +248,7 @@
         out_specs=out_specs,
         scratch_shapes=list(scratch),
     )
-    return pl.pallas_call(kernel, grid_spec=spec, out_shape=out_shape)(*scalars, *operands)
+    return pl.pallas_call(kernel, grid_spec=spec, out_shape=out_shape, compiler_params=ROOM)(*scalars, *operands)
 
 
 def permute(array, axis, pairs):
@@ -280,7 +272,9 @@
             for sign, pairs in ((-1, forward), (1, backward)):
                 chunks[sign * step][part] = permute(chunks[sign * (step - 1)][part], axis, pairs)
     last = size // 2
-    chunks[last] = (permute(chunks[1 - last][0], axis, forward), permute(chunks[last - 1][1], axis, backward))
+    chunks[last] = (
+        permute(chunks[1 - last][0], axis, forward), permute(chunks[last - 1][1], axis, backward)
+    )
     return chunks
 
 
@@ -296,12 +290,11 @@
 
 def carried_states(given, kept, axis, odd):
     size = lax.axis_size(axis)
-    like = jax.ShapeDtypeStruct(kept.shape, kept.dtype)
     other = swap(given, axis, 1)
-    pair = pl.pallas_call(pair_kernel, out_shape=like, in_specs=[smem(), vmem(), vmem()], out_specs=vmem(), name="pair")(odd, kept, other)
+    (pair,) = small(pair_kernel, (odd,), (kept, other), [(kept.shape, bf16)])
 
     def combine(earlier, later):
-        return pl.pallas_call(combine_kernel, out_shape=like, in_specs=[vmem(), vmem()], out_specs=vmem(), name="combine")(earlier, later)
+        return small(combine_kernel, (), (earlier, later), [(later.shape, bf16)])[0]
 
     earlier, later = shift(pair, axis, 2), None
     reach = 2
@@ -309,14 +302,8 @@
         before = earlier if later is None else combine(earlier, later)
         earlier, later = shift(combine(before, pair), axis, 2 * reach), before
         reach *= 2
-    state = jax.ShapeDtypeStruct((kept.shape[0], HEAD_DIM, HEAD_DIM), bf16)
-    mine, theirs = pl.pallas_call(
-        carry_kernel,
-        out_shape=(state, state),
-        in_specs=[smem()] + [vmem()] * 4,
-        out_specs=(vmem(), vmem()),
-        name="carry",
-    )(odd, earlier, later, kept, other)
+    state = ((kept.shape[0], HEAD_DIM, HEAD_DIM), bf16)
+    mine, theirs = small(carry_kernel, (odd,), (earlier, later, kept, other), [state, state])
     return mine, swap(theirs, axis, 1)
 
 
@@ -362,10 +349,10 @@
             states_kernel,
             (first, tp_at),
             (forget_logits, value_inputs, surge_log_decay, gap),
-            (wide, jax.ShapeDtypeStruct((group, HEAD_DIM + EXTRA, HEAD_DIM), bf16)),
+            (wide, pltpu.VMEM((group, HEAD_DIM + EXTRA, HEAD_DIM), bf16)),
             (steps,),
             [block, block, pl.BlockSpec((heads, rows), lambda s, first, at: (0, 0)), gap_block],
-            (own_block, pl.BlockSpec((per, HEAD_DIM + EXTRA, HEAD_DIM), lambda s, first, at: (s, 0, 0))),
+            (own_block, vmem()),
             [pltpu.VMEM((rows, heads), f32)],
         )
 
@@ -385,13 +372,13 @@
         return call(
             mix_kernel,
             (first,),
-            (local, reach, carried, output_gate_logits, head_norm_gain.reshape(1, HEAD_DIM)),
+            (local, reach, resident(carried), output_gate_logits, head_norm_gain.reshape(1, HEAD_DIM)),
             narrow,
             (steps,),
             [
                 shared,
                 shared,
-                pl.BlockSpec((per, HEAD_DIM, HEAD_DIM), lambda s, first: (s, 0, 0)),
+                vmem(),
                 pl.BlockSpec((rows, per * HEAD_DIM), lambda s, first: (0, first[0] + s)),
                 pl.BlockSpec((1, HEAD_DIM), lambda s, first: (0, 0)),
             ],
@@ -404,7 +391,9 @@
     mine, others = carried_states(given, kept, "sp", odd)
     kept_local = group_local(kept_first, kept_running)
     given_local = group_local(given_first, given_running)
-    pieces = {0: [group_mix(kept_first, *kept_local, mine), group_mix(given_first, *given_local, others)]}
+    pieces = {
+        0: [group_mix(kept_first, *kept_local, mine), group_mix(given_first, *given_local, others)]
+    }
     bit = tp // 2
     while bit:
         for rel in sorted(pieces):
@@ -412,50 +401,22 @@
         bit //= 2
     mixed = [piece for rel in range(tp) for piece in pieces[rel]]
 
-    tile = min(TILE, out_cols)
-    grid = (out_cols // tile,)
     if ringed:
-        last = sp // 2
-        cols = group * HEAD_DIM
-        chunk = cols // 2
-        partial_sum = jax.ShapeDtypeStruct((rows, out_cols), f32)
-        piece_spec = lambda: pl.BlockSpec((rows, cols), lambda n, *_: (0, 0))
-        slab = pl.BlockSpec((chunk, tile), lambda n, *_: (0, n))
-        sheet = pl.BlockSpec((rows, tile), lambda n, *_: (0, n))
-        whole_table = pl.BlockSpec((sp, rows, cols), lambda n, *_: (0, 0, 0))
-        near = [0] + [s * k for k in range(1, last - 1) for s in (-1, 1)]
-        far = [s * (last - 1) for s in (-1, 1)]
-        partial, table = call(
-            functools.partial(near_kernel, offsets=near, size=sp, n_mixed=len(mixed)),
+        offsets = [0] + [s * k for k in range(1, sp // 2) for s in (-1, 1)]
+        operands = [*mixed, *[half for off in offsets for half in chunks[off]]]
+        columns = group * HEAD_DIM
+        partial, piece = small(
+            functools.partial(project_kernel, offsets=offsets, size=sp, n_mixed=len(mixed)),
             (sp_at, tp_at),
-            (*mixed, *[half for off in near for half in chunks[off]]),
-            (partial_sum, jax.ShapeDtypeStruct((sp, rows, cols), bf16)),
-            grid,
-            [piece_spec()] * len(mixed) + [slab] * (2 * len(near)),
-            (sheet, whole_table),
+            operands,
+            [((rows, out_cols), f32), ((rows, columns), bf16)],
+            [pltpu.VMEM((sp, rows, columns), bf16)],
         )
-        partial = call(
-            functools.partial(far_kernel, offsets=far, size=sp),
-            (sp_at,),
-            (table, partial, *[half for off in far for half in chunks[off]]),
-            partial_sum,
-            grid,
-            [whole_table, sheet] + [slab] * (2 * len(far)),
-            sheet,
-        )
-        projected, squares = call(
-            functools.partial(last_kernel, size=sp),
-            (sp_at,),
-            (table, partial, *chunks[last]),
-            (jax.ShapeDtypeStruct((rows, out_cols), bf16), jax.ShapeDtypeStruct((1, rows), f32)),
-            grid,
-            [
-                pl.BlockSpec((1, rows, cols), lambda n, at: (ring_at((place_of(at[0], sp) + last) % sp, sp), 0, 0)),
-                sheet,
-                slab,
-                slab,
-            ],
-            (sheet, pl.BlockSpec((1, rows), lambda n, at: (0, 0))),
+        projected, squares = small(
+            last_kernel,
+            (),
+            (partial, piece, *chunks[sp // 2]),
+            [((rows, out_cols), bf16), ((1, rows), f32)],
             [pltpu.VMEM((rows, 128), f32)],
         )
     else:
@@ -467,18 +428,19 @@
         branch = lax.optimization_barrier(projected).astype(f32)
         squares = jnp.sum(branch * branch, axis=1)[None]
     squares = lax.psum(squares, "tp")
-    sheet = pl.BlockSpec((rows, tile), lambda n, at: (0, n))
+    tile = rows // 4
+    sheet = pl.BlockSpec((tile, out_cols), lambda n, at: (n, 0))
     return call(
         functools.partial(norm_kernel, width=width),
         (tp_at,),
         (squares, projected, residual, branch_norm_gain.reshape(1, -1)),
         jax.ShapeDtypeStruct((rows, out_cols), bf16),
-        grid,
+        (rows // tile,),
         [
-            pl.BlockSpec((1, rows), lambda n, at: (0, 0)),
+            pl.BlockSpec((1, tile), lambda n, at: (0, n)),
             sheet,
             sheet,
-            pl.BlockSpec((1, tile), lambda n, at: (0, at[0] * (out_cols // tile) + n)),
+            pl.BlockSpec((1, out_cols), lambda n, at: (0, at[0])),
         ],
         sheet,
     )
@@ -497,4 +459,6 @@
         P(),
         P("sp", "tp"),
     )
-    return jax.shard_map(layer, mesh=mesh, in_specs=placed, out_specs=P("sp", "tp"), check_vma=False)
+    return jax.shard_map(
+        layer, mesh=mesh, in_specs=placed, out_specs=P("sp", "tp"), check_vma=False
+    )

time: 135 us -> 120 us (0.89)
  Pallas kernels: 52.5 us -> 19.7 us
  waiting for transfers between devices: 37.4 us -> 57.3 us
  starting transfers between devices: 34.8 us -> 32.4 us
    pallas_call x13 -> x12, Pallas kernels: 52.5 us -> 19.7 us  [the longest x7 14.2 us: call(): pl.pallas_call(kernel, grid_spec=spec, out_shape=out_shape, compiler_para...]
    ppermute x24, waiting for transfers between devices: 37.4 us -> 57.3 us  [permute(): return lax.ppermute(array, axis, pairs)]
    ppermute x24, starting transfers between devices: 34.8 us -> 32.4 us  [permute(): return lax.ppermute(array, axis, pairs)]
    unnamed x38 -> x26, local copies, waits for them, and re-layouts: 2.83 us -> 3.94 us
  transfers between devices with their start and end apart: 24 -> 24, of which waited for: 10 -> 16; matrix products, arithmetic and copies ran while one was open for 0% -> 0% of each run, Pallas kernels for 27% -> 12%
where the time goes in v2:
time: 120 us; the launch traced here: 119 us
  waiting for transfers between devices  57.3 us (48%)
  starting transfers between devices  32.4 us (27%)
  Pallas kernels  19.7 us (16%)
  blocking collectives  5.67 us (5%)
  local copies, waits for them, and re-layouts  4.01 us (3%)
    ppermute x24, waiting for transfers between devices, permute(): return lax.ppermute(array, axis, pairs)  57.3 us
    ppermute x24, starting transfers between devices, permute(): return lax.ppermute(array, axis, pairs)  32.4 us
    pallas_call x7, Pallas kernels, call(): pl.pallas_call(kernel, grid_spec=spec, out_shape=out_shape, compiler_para...  14.2 us
    psum x1, blocking collectives, layer(): squares = lax.psum(squares, 'tp')  5.67 us
    pallas_call x5, Pallas kernels, small(): pl.pallas_call(kernel, out_shape=tuple((pltpu.VMEM(*out) for out in outs)...  5.46 us
    unnamed x26, local copies, waits for them, and re-layouts  3.94 us
  transfers between devices with their start and end apart: 24, of which 16 were waited for; matrix products, arithmetic and copies ran while one was open for 0% of the time, Pallas kernels for 12%

profile of v2, /device:TPU:0, one launch (start us, length us, event | category | flops | bytes accessed | tf_op | source)
XLA Modules:
  0.0 119.3 jit_solution(17240037165172108200)
XLA Ops:
  0.0 1.2 %copy-done = bf16[512,1024]{1,0:T(8,128)(2,1)S(1)} copy-done((bf16[512,1024]{1,0:T(8,128)(2,1)S(1)}, bf16[512,1024]{1,0:T(8,128)(2,1)}, u32[]{:S(2)}) %copy-start) | copy-done | bytes 1048600
  1.2 1.2 %copy-done.2 = bf16[512,1024]{1,0:T(8,128)(2,1)S(1)} copy-done((bf16[512,1024]{1,0:T(8,128)(2,1)S(1)}, bf16[512,1024]{1,0:T(8,128)(2,1)}, u32[]{:S(2)}) %copy-start.2) | copy-done | bytes 1048600
  3.9 2.3 %shard_map.102 = (f32[512,512]{1,0:T(8,128)S(1)}, bf16[4,136,128]{2,1,0:T(8,128)(2,1)S(1)}) custom-call(s32[1]{0:T(128)S(6)} %mul.7.first_ref, s32[1]{0:T(128)} %bitcast.tp_ref, bf16[512,1024]{1,0:T(8,128)(2,1)S(1)} %copy-done, bf16[512,1024]{1,0:T(8,128)(2,1)S(1)} %copy-done.2, f32[8,512]{1,0:T(8,128)S(1)} %copy-done.9, f32[32,1,128]{2,1,0:T(1,128)S(1)} %bitcast.5), custom_call_target="tpu_custom_call" | custom-call | tf_op jit(solution)/shard_map/pallas_call | solution.py:251
  6.2 3.0 %collective-permute-start = (bf16[4,136,128]{2,1,0:T(8,128)(2,1)S(1)}, bf16[4,136,128]{2,1,0:T(8,128)(2,1)S(1)}, u32[]{:S(2)}, u32[]{:S(2)}) collective-permute-start(bf16[4,136,128]{2,1,0:T(8,128)(2,1)S(1)} %get-tuple-element.23), channel_id=1, source_target_pairs={{0,4},{4,0},{8,12},{12,8},{16,20},{20,16},{24,28},{28,24},{1,5},{5... | collective-permute-start | bytes 417800 | tf_op jit(solution)/shard_map/ppermute | solution.py:255
  9.2 2.3 %shard_map.100 = (f32[512,512]{1,0:T(8,128)S(1)}, bf16[4,136,128]{2,1,0:T(8,128)(2,1)S(1)}) custom-call(s32[1]{0:T(128)S(6)} %mul.6.first_ref, s32[1]{0:T(128)} %bitcast.tp_ref, bf16[512,1024]{1,0:T(8,128)(2,1)S(1)} %copy-done.1, bf16[512,1024]{1,0:T(8,128)(2,1)S(1)} %copy-done.2, f32[8,512]{1,0:T(8,128)S(1)} %copy-done.9, f32[32,1,128]{2,1,0:T(1,128)S(1)} %bitcast.6), custom_call_target="tpu_custom_call" | custom-call | tf_op jit(solution)/shard_map/pallas_call | solution.py:251
  11.5 1.4 %collective-permute-done.other_ref = bf16[4,136,128]{2,1,0:T(8,128)(2,1)S(1)} collective-permute-done((bf16[4,136,128]{2,1,0:T(8,128)(2,1)S(1)}, bf16[4,136,128]{2,1,0:T(8,128)(2,1)S(1)}, u32[]{:S(2)}, u32[]{:S(2)}) %collective-permute-start) | collective-permute-done | bytes 139296 | tf_op jit(solution)/shard_map/ppermute | solution.py:255
  13.0 3.7 %collective-permute-start.1 = (bf16[4,136,128]{2,1,0:T(8,128)(2,1)S(1)}, bf16[4,136,128]{2,1,0:T(8,128)(2,1)S(1)}, u32[]{:S(2)}, u32[]{:S(2)}) collective-permute-start(bf16[4,136,128]{2,1,0:T(8,128)(2,1)S(1)} %shard_map.103.later_ref), channel_id=1, source_target_pairs={{0,8},{4,12},{8,16},{12,20},{16,24},{20,28},{1,9},{5,13},{9,17},{1... | collective-permute-start | bytes 417800 | tf_op jit(solution)/shard_map/ppermute | solution.py:255
  16.7 2.6 %collective-permute-done.1.earlier_ref.later_ref = bf16[4,136,128]{2,1,0:T(8,128)(2,1)S(1)} collective-permute-done((bf16[4,136,128]{2,1,0:T(8,128)(2,1)S(1)}, bf16[4,136,128]{2,1,0:T(8,128)(2,1)S(1)}, u32[]{:S(2)}, u32[]{:S(2)}) %collective-permute-start.1) | collective-permute-done | bytes 139296 | tf_op jit(solution)/shard_map/ppermute | solution.py:255
  19.3 5.4 %collective-permute-start.2 = (bf16[4,136,128]{2,1,0:T(8,128)(2,1)S(1)}, bf16[4,136,128]{2,1,0:T(8,128)(2,1)S(1)}, u32[]{:S(2)}, u32[]{:S(2)}) collective-permute-start(bf16[4,136,128]{2,1,0:T(8,128)(2,1)S(1)} %shard_map.104), channel_id=1, source_target_pairs={{0,16},{4,20},{8,24},{12,28},{1,17},{5,21},{9,25},{13,29},{2,18},{... | collective-permute-start | bytes 417800 | tf_op jit(solution)/shard_map/ppermute | solution.py:255
  24.8 1.6 %collective-permute-start.10 = (bf16[256,1024]{1,0:T(8,128)(2,1)S(1)}, bf16[256,1024]{1,0:T(8,128)(2,1)S(1)}, u32[]{:S(2)}, u32[]{:S(2)}) collective-permute-start(bf16[256,1024]{1,0:T(8,128)(2,1)S(1)} %get-tuple-element.34.refs_8_), channel_id=1, source_target_pairs={{0,8},{8,16},{16,24},{24,28},{28,20},{20,12},{12,4},{4,0},{1,9},{9... | collective-permute-start | bytes 1572872 | tf_op jit(solution)/shard_map/ppermute | solution.py:255
  26.9 1.6 %collective-permute-start.11 = (bf16[256,1024]{1,0:T(8,128)(2,1)S(1)}, bf16[256,1024]{1,0:T(8,128)(2,1)S(1)}, u32[]{:S(2)}, u32[]{:S(2)}) collective-permute-start(bf16[256,1024]{1,0:T(8,128)(2,1)S(1)} %get-tuple-element.33.refs_9_), channel_id=1, source_target_pairs={{0,8},{8,16},{16,24},{24,28},{28,20},{20,12},{12,4},{4,0},{1,9},{9... | collective-permute-start | bytes 1572872 | tf_op jit(solution)/shard_map/ppermute | solution.py:255
  28.9 2.6 %shard_map.101 = (f32[512,512]{1,0:T(8,128)S(1)}, bf16[512,512]{1,0:T(8,128)(2,1)S(1)}) custom-call(s32[1]{0:T(128)S(6)} %mul.6.first_ref, s32[1]{0:T(128)} %bitcast.tp_ref, bf16[512,1024]{1,0:T(8,128)(2,1)S(1)} %copy-done.4, bf16[512,1024]{1,0:T(8,128)(2,1)S(1)} %copy-done.1, bf16[512,1024]{1,0:T(8,128)(2,1)S(1)} %copy-done.2, ...), custom_call_target="tpu_custom_call" | custom-call | tf_op jit(solution)/shard_map/pallas_call | solution.py:251
  32.9 1.6 %collective-permute-start.6 = (bf16[512,512]{1,0:T(8,128)(2,1)S(1)}, bf16[512,512]{1,0:T(8,128)(2,1)S(1)}, u32[]{:S(2)}, u32[]{:S(2)}) collective-permute-start(bf16[512,512]{1,0:T(8,128)(2,1)S(1)} %shard_map.106.refs_0_), channel_id=1, source_target_pairs={{0,2},{1,3},{2,0},{3,1},{4,6},{5,7},{6,4},{7,5},{8,10},{9,11},{10,... | collective-permute-start | bytes 1572872 | tf_op jit(solution)/shard_map/ppermute | solution.py:255
  34.5 5.5 %collective-permute-done.10.refs_10_ = bf16[256,1024]{1,0:T(8,128)(2,1)S(1)} collective-permute-done((bf16[256,1024]{1,0:T(8,128)(2,1)S(1)}, bf16[256,1024]{1,0:T(8,128)(2,1)S(1)}, u32[]{:S(2)}, u32[]{:S(2)}) %collective-permute-start.10) | collective-permute-done | bytes 524320 | tf_op jit(solution)/shard_map/ppermute | solution.py:255
  41.2 8.9 %collective-permute-done.11.refs_11_ = bf16[256,1024]{1,0:T(8,128)(2,1)S(1)} collective-permute-done((bf16[256,1024]{1,0:T(8,128)(2,1)S(1)}, bf16[256,1024]{1,0:T(8,128)(2,1)S(1)}, u32[]{:S(2)}, u32[]{:S(2)}) %collective-permute-start.11) | collective-permute-done | bytes 524320 | tf_op jit(solution)/shard_map/ppermute | solution.py:255
  50.1 2.5 %collective-permute-start.14 = (bf16[256,1024]{1,0:T(8,128)(2,1)S(1)}, bf16[256,1024]{1,0:T(8,128)(2,1)S(1)}, u32[]{:S(2)}, u32[]{:S(2)}) collective-permute-start(bf16[256,1024]{1,0:T(8,128)(2,1)S(1)} %collective-permute-done.10.refs_10_), channel_id=1, source_target_pairs={{0,8},{8,16},{16,24},{24,28},{28,20},{20,12},{12,4},{4,0},{1,9},{9... | collective-permute-start | bytes 1572872 | tf_op jit(solution)/shard_map/ppermute | solution.py:255
  52.9 2.2 %collective-permute-start.15 = (bf16[256,1024]{1,0:T(8,128)(2,1)S(1)}, bf16[256,1024]{1,0:T(8,128)(2,1)S(1)}, u32[]{:S(2)}, u32[]{:S(2)}) collective-permute-start(bf16[256,1024]{1,0:T(8,128)(2,1)S(1)} %collective-permute-done.11.refs_11_), channel_id=1, source_target_pairs={{0,8},{8,16},{16,24},{24,28},{28,20},{20,12},{12,4},{4,0},{1,9},{9... | collective-permute-start | bytes 1572872 | tf_op jit(solution)/shard_map/ppermute | solution.py:255
  55.1 2.6 %shard_map.107 = (f32[512,512]{1,0:T(8,128)S(1)}, bf16[512,512]{1,0:T(8,128)(2,1)S(1)}) custom-call(s32[1]{0:T(128)S(6)} %mul.7.first_ref, s32[1]{0:T(128)} %bitcast.tp_ref, bf16[512,1024]{1,0:T(8,128)(2,1)S(1)} %copy-done.4, bf16[512,1024]{1,0:T(8,128)(2,1)S(1)} %copy-done.1, bf16[512,1024]{1,0:T(8,128)(2,1)S(1)} %copy-done.3, ...), custom_call_target="tpu_custom_call" | custom-call | tf_op jit(solution)/shard_map/pallas_call | solution.py:251
  59.0 1.6 %collective-permute-start.7 = (bf16[512,512]{1,0:T(8,128)(2,1)S(1)}, bf16[512,512]{1,0:T(8,128)(2,1)S(1)}, u32[]{:S(2)}, u32[]{:S(2)}) collective-permute-start(bf16[512,512]{1,0:T(8,128)(2,1)S(1)} %shard_map.108.refs_1_), channel_id=1, source_target_pairs={{0,2},{1,3},{2,0},{3,1},{4,6},{5,7},{6,4},{7,5},{8,10},{9,11},{10,... | collective-permute-start | bytes 1572872 | tf_op jit(solution)/shard_map/ppermute | solution.py:255
  60.5 4.4 %collective-permute-done.14.refs_14_ = bf16[256,1024]{1,0:T(8,128)(2,1)S(1)} collective-permute-done((bf16[256,1024]{1,0:T(8,128)(2,1)S(1)}, bf16[256,1024]{1,0:T(8,128)(2,1)S(1)}, u32[]{:S(2)}, u32[]{:S(2)}) %collective-permute-start.14) | collective-permute-done | bytes 524320 | tf_op jit(solution)/shard_map/ppermute | solution.py:255
  64.9 2.9 %collective-permute-done.17.refs_17_ = bf16[256,1024]{1,0:T(8,128)(2,1)S(1)} collective-permute-done((bf16[256,1024]{1,0:T(8,128)(2,1)S(1)}, bf16[256,1024]{1,0:T(8,128)(2,1)S(1)}, u32[]{:S(2)}, u32[]{:S(2)}) %collective-permute-start.17) | collective-permute-done | bytes 524320 | tf_op jit(solution)/shard_map/ppermute | solution.py:255
  67.8 5.8 %collective-permute-done.15.refs_15_ = bf16[256,1024]{1,0:T(8,128)(2,1)S(1)} collective-permute-done((bf16[256,1024]{1,0:T(8,128)(2,1)S(1)}, bf16[256,1024]{1,0:T(8,128)(2,1)S(1)}, u32[]{:S(2)}, u32[]{:S(2)}) %collective-permute-start.15) | collective-permute-done | bytes 524320 | tf_op jit(solution)/shard_map/ppermute | solution.py:255
  73.6 2.5 %collective-permute-start.18 = (bf16[256,1024]{1,0:T(8,128)(2,1)S(1)}, bf16[256,1024]{1,0:T(8,128)(2,1)S(1)}, u32[]{:S(2)}, u32[]{:S(2)}) collective-permute-start(bf16[256,1024]{1,0:T(8,128)(2,1)S(1)} %collective-permute-done.14.refs_14_), channel_id=1, source_target_pairs={{0,8},{8,16},{16,24},{24,28},{28,20},{20,12},{12,4},{4,0},{1,9},{9... | collective-permute-start | bytes 1572872 | tf_op jit(solution)/shard_map/ppermute | solution.py:255
  76.6 2.1 %collective-permute-start.19 = (bf16[256,1024]{1,0:T(8,128)(2,1)S(1)}, bf16[256,1024]{1,0:T(8,128)(2,1)S(1)}, u32[]{:S(2)}, u32[]{:S(2)}) collective-permute-start(bf16[256,1024]{1,0:T(8,128)(2,1)S(1)} %collective-permute-done.15.refs_15_), channel_id=1, source_target_pairs={{0,8},{8,16},{16,24},{24,28},{28,20},{20,12},{12,4},{4,0},{1,9},{9... | collective-permute-start | bytes 1572872 | tf_op jit(solution)/shard_map/ppermute | solution.py:255
  78.7 9.7 %collective-permute-done.18.refs_18_ = bf16[256,1024]{1,0:T(8,128)(2,1)S(1)} collective-permute-done((bf16[256,1024]{1,0:T(8,128)(2,1)S(1)}, bf16[256,1024]{1,0:T(8,128)(2,1)S(1)}, u32[]{:S(2)}, u32[]{:S(2)}) %collective-permute-start.18) | collective-permute-done | bytes 524320 | tf_op jit(solution)/shard_map/ppermute | solution.py:255
  88.4 2.5 %collective-permute-start.22 = (bf16[256,1024]{1,0:T(8,128)(2,1)S(1)}, bf16[256,1024]{1,0:T(8,128)(2,1)S(1)}, u32[]{:S(2)}, u32[]{:S(2)}) collective-permute-start(bf16[256,1024]{1,0:T(8,128)(2,1)S(1)} %collective-permute-done.18.refs_18_), channel_id=1, source_target_pairs={{0,8},{8,16},{16,24},{24,28},{28,20},{20,12},{12,4},{4,0},{1,9},{9... | collective-permute-start | bytes 1572872 | tf_op jit(solution)/shard_map/ppermute | solution.py:255
  91.4 8.3 %collective-permute-done.19.refs_19_ = bf16[256,1024]{1,0:T(8,128)(2,1)S(1)} collective-permute-done((bf16[256,1024]{1,0:T(8,128)(2,1)S(1)}, bf16[256,1024]{1,0:T(8,128)(2,1)S(1)}, u32[]{:S(2)}, u32[]{:S(2)}) %collective-permute-start.19) | collective-permute-done | bytes 524320 | tf_op jit(solution)/shard_map/ppermute | solution.py:255
  99.7 2.9 %collective-permute-done.20.refs_20_ = bf16[256,1024]{1,0:T(8,128)(2,1)S(1)} collective-permute-done((bf16[256,1024]{1,0:T(8,128)(2,1)S(1)}, bf16[256,1024]{1,0:T(8,128)(2,1)S(1)}, u32[]{:S(2)}, u32[]{:S(2)}) %collective-permute-start.20) | collective-permute-done | bytes 524320 | tf_op jit(solution)/shard_map/ppermute | solution.py:255
  102.6 4.2 %shard_map.109 = (f32[512,1024]{1,0:T(8,128)S(1)}, bf16[512,512]{1,0:T(8,128)(2,1)S(1)}) custom-call(s32[1]{0:T(128)} %bitcast.1.sp_ref, s32[1]{0:T(128)} %bitcast.tp_ref, bf16[512,512]{1,0:T(8,128)(2,1)S(1)} %shard_map.106.refs_0_, bf16[512,512]{1,0:T(8,128)(2,1)S(1)} %shard_map.108.refs_1_, bf16[512,512]{1,0:T(8,128)(2,1)S(1)} %collective-permute-done.4.refs_2_, ...), custom_call_target="tpu_custom_call" | custom-call | tf_op jit(solution)/shard_map/pallas_call | solution.py:233
  107.5 2.9 %collective-permute-done.23.second_ref = bf16[256,1024]{1,0:T(8,128)(2,1)S(1)} collective-permute-done((bf16[256,1024]{1,0:T(8,128)(2,1)S(1)}, bf16[256,1024]{1,0:T(8,128)(2,1)S(1)}, u32[]{:S(2)}, u32[]{:S(2)}) %collective-permute-start.23) | collective-permute-done | bytes 524320 | tf_op jit(solution)/shard_map/ppermute | solution.py:255
  111.4 5.7 %psum.7.square_ref = f32[1,512]{1,0:T(1,128)S(1)} all-reduce(f32[1,512]{1,0:T(1,128)S(1)} %get-tuple-element.31), channel_id=1, replica_groups=mesh['sp'=8,'tp'=4] {'tp'}, use_global_device_ids=true, to_apply=%region_0.1 | all-reduce | flops 512 | bytes 4096 | tf_op jit(solution)/shard_map/psum | solution.py:430
  117.1 2.2 %shard_map.111 = bf16[512,1024]{1,0:T(8,128)(2,1)} custom-call(s32[1]{0:T(128)} %bitcast.tp_ref, f32[1,512]{1,0:T(1,128)S(1)} %psum.7.square_ref, bf16[512,1024]{1,0:T(8,128)(2,1)S(1)} %get-tuple-element.32.projected_ref, bf16[512,1024]{1,0:T(8,128)(2,1)S(1)} %copy-done.6, f32[1,4096]{1,0:T(1,128)S(1)} %bitcast.9), custom_call_target="tpu_custom_call" | custom-call | tf_op jit(solution)/shard_map/pallas_call | solution.py:251
  (56 shorter events, 9.3 us)
Async XLA Ops:
  0.0 9.2 %copy-start.8 = (f32[4096]{0:T(1024)S(1)}, f32[4096]{0:T(1024)}, u32[]{:S(2)}) copy-start(f32[4096]{0:T(1024)} %param.14) | copy-start | bytes 49156
  3.9 5.3 %copy-start.1 = (bf16[512,1024]{1,0:T(8,128)(2,1)S(1)}, bf16[512,1024]{1,0:T(8,128)(2,1)}, u32[]{:S(2)}) copy-start(bf16[512,1024]{1,0:T(8,128)(2,1)} %forget_ref.7) | copy-start | bytes 3145732
  3.9 20.8 %copy-start.12 = (bf16[512,1024]{1,0:T(8,128)(2,1)S(1)}, bf16[512,1024]{1,0:T(8,128)(2,1)}, u32[]{:S(2)}) copy-start(bf16[512,1024]{1,0:T(8,128)(2,1)} %param.17) | copy-start | bytes 3145732
  6.2 6.7 %collective-permute-start = (bf16[4,136,128]{2,1,0:T(8,128)(2,1)S(1)}, bf16[4,136,128]{2,1,0:T(8,128)(2,1)S(1)}, u32[]{:S(2)}, u32[]{:S(2)}) collective-permute-start(bf16[4,136,128]{2,1,0:T(8,128)(2,1)S(1)} %get-tuple-element.23), channel_id=1, source_target_pairs={{0,4},{4,0},{8,12},{12,8},{16,20},{20,16},{24,28},{28,24},{1,5},{5... | collective-permute-start | bytes 417800 | tf_op jit(solution)/shard_map/ppermute | solution.py:255
  9.2 19.7 %copy-start.4 = (bf16[512,1024]{1,0:T(8,128)(2,1)S(1)}, bf16[512,1024]{1,0:T(8,128)(2,1)}, u32[]{:S(2)}) copy-start(bf16[512,1024]{1,0:T(8,128)(2,1)} %query_ref.3) | copy-start | bytes 3145732
  13.0 6.3 %collective-permute-start.1 = (bf16[4,136,128]{2,1,0:T(8,128)(2,1)S(1)}, bf16[4,136,128]{2,1,0:T(8,128)(2,1)S(1)}, u32[]{:S(2)}, u32[]{:S(2)}) collective-permute-start(bf16[4,136,128]{2,1,0:T(8,128)(2,1)S(1)} %shard_map.103.later_ref), channel_id=1, source_target_pairs={{0,8},{4,12},{8,16},{12,20},{16,24},{20,28},{1,9},{5,13},{9,17},{1... | collective-permute-start | bytes 417800 | tf_op jit(solution)/shard_map/ppermute | solution.py:255
  19.3 12.2 %collective-permute-start.2 = (bf16[4,136,128]{2,1,0:T(8,128)(2,1)S(1)}, bf16[4,136,128]{2,1,0:T(8,128)(2,1)S(1)}, u32[]{:S(2)}, u32[]{:S(2)}) collective-permute-start(bf16[4,136,128]{2,1,0:T(8,128)(2,1)S(1)} %shard_map.104), channel_id=1, source_target_pairs={{0,16},{4,20},{8,24},{12,28},{1,17},{5,21},{9,25},{13,29},{2,18},{... | collective-permute-start | bytes 417800 | tf_op jit(solution)/shard_map/ppermute | solution.py:255
  24.8 15.2 %collective-permute-start.10 = (bf16[256,1024]{1,0:T(8,128)(2,1)S(1)}, bf16[256,1024]{1,0:T(8,128)(2,1)S(1)}, u32[]{:S(2)}, u32[]{:S(2)}) collective-permute-start(bf16[256,1024]{1,0:T(8,128)(2,1)S(1)} %get-tuple-element.34.refs_8_), channel_id=1, source_target_pairs={{0,8},{8,16},{16,24},{24,28},{28,20},{20,12},{12,4},{4,0},{1,9},{9... | collective-permute-start | bytes 1572872 | tf_op jit(solution)/shard_map/ppermute | solution.py:255
  26.4 14.8 %collective-permute-start.13 = (bf16[256,1024]{1,0:T(8,128)(2,1)S(1)}, bf16[256,1024]{1,0:T(8,128)(2,1)S(1)}, u32[]{:S(2)}, u32[]{:S(2)}) collective-permute-start(bf16[256,1024]{1,0:T(8,128)(2,1)S(1)} %get-tuple-element.33.refs_9_), channel_id=1, source_target_pairs={{8,0},{16,8},{24,16},{28,24},{20,28},{12,20},{4,12},{0,4},{9,1},{1... | collective-permute-start | bytes 1572872 | tf_op jit(solution)/shard_map/ppermute | solution.py:255
  26.9 23.2 %collective-permute-start.11 = (bf16[256,1024]{1,0:T(8,128)(2,1)S(1)}, bf16[256,1024]{1,0:T(8,128)(2,1)S(1)}, u32[]{:S(2)}, u32[]{:S(2)}) collective-permute-start(bf16[256,1024]{1,0:T(8,128)(2,1)S(1)} %get-tuple-element.33.refs_9_), channel_id=1, source_target_pairs={{0,8},{8,16},{16,24},{24,28},{28,20},{20,12},{12,4},{4,0},{1,9},{9... | collective-permute-start | bytes 1572872 | tf_op jit(solution)/shard_map/ppermute | solution.py:255
  28.5 24.1 %collective-permute-start.12 = (bf16[256,1024]{1,0:T(8,128)(2,1)S(1)}, bf16[256,1024]{1,0:T(8,128)(2,1)S(1)}, u32[]{:S(2)}, u32[]{:S(2)}) collective-permute-start(bf16[256,1024]{1,0:T(8,128)(2,1)S(1)} %get-tuple-element.34.refs_8_), channel_id=1, source_target_pairs={{8,0},{16,8},{24,16},{28,24},{20,28},{12,20},{4,12},{0,4},{9,1},{1... | collective-permute-start | bytes 1572872 | tf_op jit(solution)/shard_map/ppermute | solution.py:255
  28.9 2.8 %copy-start.11 = (f32[128]{0:T(128)S(1)}, f32[128]{0:T(128)}, u32[]{:S(2)}) copy-start(f32[128]{0:T(128)} %param.16) | copy-start | bytes 1540
  31.5 23.6 %copy-start.3 = (bf16[512,1024]{1,0:T(8,128)(2,1)S(1)}, bf16[512,1024]{1,0:T(8,128)(2,1)}, u32[]{:S(2)}) copy-start(bf16[512,1024]{1,0:T(8,128)(2,1)} %value_ref.7) | copy-start | bytes 3145732
  32.9 22.3 %collective-permute-start.6 = (bf16[512,512]{1,0:T(8,128)(2,1)S(1)}, bf16[512,512]{1,0:T(8,128)(2,1)S(1)}, u32[]{:S(2)}, u32[]{:S(2)}) collective-permute-start(bf16[512,512]{1,0:T(8,128)(2,1)S(1)} %shard_map.106.refs_0_), channel_id=1, source_target_pairs={{0,2},{1,3},{2,0},{3,1},{4,6},{5,7},{6,4},{7,5},{8,10},{9,11},{10,... | collective-permute-start | bytes 1572872 | tf_op jit(solution)/shard_map/ppermute | solution.py:255
  40.0 12.9 %collective-permute-start.3 = (bf16[4,128,128]{2,1,0:T(8,128)(2,1)S(1)}, bf16[4,128,128]{2,1,0:T(8,128)(2,1)S(1)}, u32[]{:S(2)}, u32[]{:S(2)}) collective-permute-start(bf16[4,128,128]{2,1,0:T(8,128)(2,1)S(1)} %get-tuple-element.28), channel_id=1, source_target_pairs={{0,4},{4,0},{8,12},{12,8},{16,20},{20,16},{24,28},{28,24},{1,5},{5... | collective-permute-start | bytes 393224 | tf_op jit(solution)/shard_map/ppermute | solution.py:255
  41.2 17.7 %collective-permute-start.4 = (bf16[512,512]{1,0:T(8,128)(2,1)S(1)}, bf16[512,512]{1,0:T(8,128)(2,1)S(1)}, u32[]{:S(2)}, u32[]{:S(2)}) collective-permute-start(bf16[512,512]{1,0:T(8,128)(2,1)S(1)} %shard_map.106.refs_0_), channel_id=1, source_target_pairs={{0,1},{1,0},{2,3},{3,2},{4,5},{5,4},{6,7},{7,6},{8,9},{9,8},{10,11... | collective-permute-start | bytes 1572872 | tf_op jit(solution)/shard_map/ppermute | solution.py:255
  50.1 14.8 %collective-permute-start.14 = (bf16[256,1024]{1,0:T(8,128)(2,1)S(1)}, bf16[256,1024]{1,0:T(8,128)(2,1)S(1)}, u32[]{:S(2)}, u32[]{:S(2)}) collective-permute-start(bf16[256,1024]{1,0:T(8,128)(2,1)S(1)} %collective-permute-done.10.refs_10_), channel_id=1, source_target_pairs={{0,8},{8,16},{16,24},{24,28},{28,20},{20,12},{12,4},{4,0},{1,9},{9... | collective-permute-start | bytes 1572872 | tf_op jit(solution)/shard_map/ppermute | solution.py:255
  52.6 15.3 %collective-permute-start.17 = (bf16[256,1024]{1,0:T(8,128)(2,1)S(1)}, bf16[256,1024]{1,0:T(8,128)(2,1)S(1)}, u32[]{:S(2)}, u32[]{:S(2)}) collective-permute-start(bf16[256,1024]{1,0:T(8,128)(2,1)S(1)} %collective-permute-done.13.refs_13_), channel_id=1, source_target_pairs={{8,0},{16,8},{24,16},{28,24},{20,28},{12,20},{4,12},{0,4},{9,1},{1... | collective-permute-start | bytes 1572872 | tf_op jit(solution)/shard_map/ppermute | solution.py:255
  52.9 20.7 %collective-permute-start.15 = (bf16[256,1024]{1,0:T(8,128)(2,1)S(1)}, bf16[256,1024]{1,0:T(8,128)(2,1)S(1)}, u32[]{:S(2)}, u32[]{:S(2)}) collective-permute-start(bf16[256,1024]{1,0:T(8,128)(2,1)S(1)} %collective-permute-done.11.refs_11_), channel_id=1, source_target_pairs={{0,8},{8,16},{16,24},{24,28},{28,20},{20,12},{12,4},{4,0},{1,9},{9... | collective-permute-start | bytes 1572872 | tf_op jit(solution)/shard_map/ppermute | solution.py:255
  55.1 21.4 %collective-permute-start.16 = (bf16[256,1024]{1,0:T(8,128)(2,1)S(1)}, bf16[256,1024]{1,0:T(8,128)(2,1)S(1)}, u32[]{:S(2)}, u32[]{:S(2)}) collective-permute-start(bf16[256,1024]{1,0:T(8,128)(2,1)S(1)} %collective-permute-done.12.refs_12_), channel_id=1, source_target_pairs={{8,0},{16,8},{24,16},{28,24},{20,28},{12,20},{4,12},{0,4},{9,1},{1... | collective-permute-start | bytes 1572872 | tf_op jit(solution)/shard_map/ppermute | solution.py:255
  59.0 17.6 %collective-permute-start.7 = (bf16[512,512]{1,0:T(8,128)(2,1)S(1)}, bf16[512,512]{1,0:T(8,128)(2,1)S(1)}, u32[]{:S(2)}, u32[]{:S(2)}) collective-permute-start(bf16[512,512]{1,0:T(8,128)(2,1)S(1)} %shard_map.108.refs_1_), channel_id=1, source_target_pairs={{0,2},{1,3},{2,0},{3,1},{4,6},{5,7},{6,4},{7,5},{8,10},{9,11},{10,... | collective-permute-start | bytes 1572872 | tf_op jit(solution)/shard_map/ppermute | solution.py:255
  64.9 13.8 %collective-permute-start.5 = (bf16[512,512]{1,0:T(8,128)(2,1)S(1)}, bf16[512,512]{1,0:T(8,128)(2,1)S(1)}, u32[]{:S(2)}, u32[]{:S(2)}) collective-permute-start(bf16[512,512]{1,0:T(8,128)(2,1)S(1)} %shard_map.108.refs_1_), channel_id=1, source_target_pairs={{0,1},{1,0},{2,3},{3,2},{4,5},{5,4},{6,7},{7,6},{8,9},{9,8},{10,11... | collective-permute-start | bytes 1572872 | tf_op jit(solution)/shard_map/ppermute | solution.py:255
  67.8 10.8 %collective-permute-start.8 = (bf16[512,512]{1,0:T(8,128)(2,1)S(1)}, bf16[512,512]{1,0:T(8,128)(2,1)S(1)}, u32[]{:S(2)}, u32[]{:S(2)}) collective-permute-start(bf16[512,512]{1,0:T(8,128)(2,1)S(1)} %collective-permute-done.6.refs_4_), channel_id=1, source_target_pairs={{0,1},{1,0},{2,3},{3,2},{4,5},{5,4},{6,7},{7,6},{8,9},{9,8},{10,11... | collective-permute-start | bytes 1572872 | tf_op jit(solution)/shard_map/ppermute | solution.py:255
  73.6 14.8 %collective-permute-start.18 = (bf16[256,1024]{1,0:T(8,128)(2,1)S(1)}, bf16[256,1024]{1,0:T(8,128)(2,1)S(1)}, u32[]{:S(2)}, u32[]{:S(2)}) collective-permute-start(bf16[256,1024]{1,0:T(8,128)(2,1)S(1)} %collective-permute-done.14.refs_14_), channel_id=1, source_target_pairs={{0,8},{8,16},{16,24},{24,28},{28,20},{20,12},{12,4},{4,0},{1,9},{9... | collective-permute-start | bytes 1572872 | tf_op jit(solution)/shard_map/ppermute | solution.py:255
  76.6 14.8 %collective-permute-start.21 = (bf16[256,1024]{1,0:T(8,128)(2,1)S(1)}, bf16[256,1024]{1,0:T(8,128)(2,1)S(1)}, u32[]{:S(2)}, u32[]{:S(2)}) collective-permute-start(bf16[256,1024]{1,0:T(8,128)(2,1)S(1)} %collective-permute-done.17.refs_17_), channel_id=1, source_target_pairs={{8,0},{16,8},{24,16},{28,24},{20,28},{12,20},{4,12},{0,4},{9,1},{1... | collective-permute-start | bytes 1572872 | tf_op jit(solution)/shard_map/ppermute | solution.py:255
  76.6 23.1 %collective-permute-start.19 = (bf16[256,1024]{1,0:T(8,128)(2,1)S(1)}, bf16[256,1024]{1,0:T(8,128)(2,1)S(1)}, u32[]{:S(2)}, u32[]{:S(2)}) collective-permute-start(bf16[256,1024]{1,0:T(8,128)(2,1)S(1)} %collective-permute-done.15.refs_15_), channel_id=1, source_target_pairs={{0,8},{8,16},{16,24},{24,28},{28,20},{20,12},{12,4},{4,0},{1,9},{9... | collective-permute-start | bytes 1572872 | tf_op jit(solution)/shard_map/ppermute | solution.py:255
  78.7 23.9 %collective-permute-start.20 = (bf16[256,1024]{1,0:T(8,128)(2,1)S(1)}, bf16[256,1024]{1,0:T(8,128)(2,1)S(1)}, u32[]{:S(2)}, u32[]{:S(2)}) collective-permute-start(bf16[256,1024]{1,0:T(8,128)(2,1)S(1)} %collective-permute-done.16.refs_16_), channel_id=1, source_target_pairs={{8,0},{16,8},{24,16},{28,24},{20,28},{12,20},{4,12},{0,4},{9,1},{1... | collective-permute-start | bytes 1572872 | tf_op jit(solution)/shard_map/ppermute | solution.py:255
  78.7 23.9 %collective-permute-start.9 = (bf16[512,512]{1,0:T(8,128)(2,1)S(1)}, bf16[512,512]{1,0:T(8,128)(2,1)S(1)}, u32[]{:S(2)}, u32[]{:S(2)}) collective-permute-start(bf16[512,512]{1,0:T(8,128)(2,1)S(1)} %collective-permute-done.7.refs_5_), channel_id=1, source_target_pairs={{0,1},{1,0},{2,3},{3,2},{4,5},{5,4},{6,7},{7,6},{8,9},{9,8},{10,11... | collective-permute-start | bytes 1572872 | tf_op jit(solution)/shard_map/ppermute | solution.py:255
  88.4 19.1 %collective-permute-start.22 = (bf16[256,1024]{1,0:T(8,128)(2,1)S(1)}, bf16[256,1024]{1,0:T(8,128)(2,1)S(1)}, u32[]{:S(2)}, u32[]{:S(2)}) collective-permute-start(bf16[256,1024]{1,0:T(8,128)(2,1)S(1)} %collective-permute-done.18.refs_18_), channel_id=1, source_target_pairs={{0,8},{8,16},{16,24},{24,28},{28,20},{20,12},{12,4},{4,0},{1,9},{9... | collective-permute-start | bytes 1572872 | tf_op jit(solution)/shard_map/ppermute | solution.py:255
  91.4 19.1 %collective-permute-start.23 = (bf16[256,1024]{1,0:T(8,128)(2,1)S(1)}, bf16[256,1024]{1,0:T(8,128)(2,1)S(1)}, u32[]{:S(2)}, u32[]{:S(2)}) collective-permute-start(bf16[256,1024]{1,0:T(8,128)(2,1)S(1)} %collective-permute-done.21.refs_21_), channel_id=1, source_target_pairs={{8,0},{16,8},{24,16},{28,24},{20,28},{12,20},{4,12},{0,4},{9,1},{1... | collective-permute-start | bytes 1572872 | tf_op jit(solution)/shard_map/ppermute | solution.py:255
  106.8 10.3 %copy-start.6 = (bf16[512,1024]{1,0:T(8,128)(2,1)S(1)}, bf16[512,1024]{1,0:T(8,128)(2,1)}, u32[]{:S(2)}) copy-start(bf16[512,1024]{1,0:T(8,128)(2,1)} %residual_ref.1) | copy-start | bytes 3145732
  106.8 10.3 %copy-start.10 = (f32[4096]{0:T(1024)S(1)}, f32[4096]{0:T(1024)}, u32[]{:S(2)}) copy-start(f32[4096]{0:T(1024)} %param.18) | copy-start | bytes 49156
  (5 other events, 6.7 us)
